TPU v7x, 512 devices: a whole 4x4x16 slice. The times are simulated.
512 devices in a mesh: sp: 128 (over z, x, core), tp: 4 (over y).
Axes of the slice: x: 4, y: 4, z: 16, core: 2. Of those that a mesh axis runs over, the one named last changes fastest.
Arguments:
- tokens: bfloat16 [65536, 2048], P(('sp', 'tp')), may hold values from -6 to 6
- norm_gain: float32 [2048], replicated, may hold values from 0.1 to 1.9
- pool_in_weight: bfloat16 [2048, 1024], P('sp', 'tp'), may hold values from -0.125 to 0.125
- query_weight: bfloat16 [2048, 1024], P('sp', 'tp'), may hold values from -0.125 to 0.125
- forget_weight: bfloat16 [2048, 1024], P('sp', 'tp'), may hold values from -0.125 to 0.125
- input_weight: bfloat16 [2048, 1024], P('sp', 'tp'), may hold values from -0.125 to 0.125
- forget_gap: float32 [1024], P('tp'), may hold values from 0 to 0.02
- decay_shift: float32 [8, 65536], P('tp', 'sp'), may hold values from -0.42 to 0
- out_gain: float32 [128], replicated, may hold values from 0.1 to 1.9
- pool_out_weight: bfloat16 [1024, 2048], P('tp', 'sp'), may hold values from -0.53033009 to 0.53033009
- recur_out_weight: bfloat16 [1024, 2048], P('tp', 'sp'), may hold values from -0.53033009 to 0.53033009
Outputs:
- mixed_out: bfloat16 [65536, 2048], P(('sp', 'tp'))
All inputs are finite; a program needn't handle non-finite values.
Results may differ from a plain program's by a relative error of at most 0.014.
Values may be sent and summed in bfloat16 or wider, within the bound.
No kernel may reach another device: no remote copies, remote signals or barrier semaphores. Data moves between devices by JAX's collectives and lax.ppermute only.
A program may use at most 64 MiB of HBM per device.

v0:
```python
import jax
import jax.numpy as jnp
from jax import lax
from jax.experimental import pallas as pl
from jax.experimental.pallas import tpu as pltpu
from jax.sharding import Mesh
from jax.sharding import PartitionSpec as P


GROUPS = 4
RDIM = 128
CHUNK = 128
RIM = 16
FAR, NEAR, ACROSS, CORE = "sp_f", "sp_n", "sp_x", "sp_c"
DEPTH = (FAR, NEAR)
PLANE = (ACROSS, CORE)
SP = (FAR, NEAR, ACROSS, CORE)
SP_TP = (FAR, NEAR, ACROSS, CORE, "tp")
EPSILON = 1e-06
BF = jnp.bfloat16
F32 = jnp.float32
NT = (((1,), (1,)), ((), ()))
TN = (((0,), (0,)), ((), ()))
NN = (((1,), (0,)), ((), ()))


def dot(a, b, dims=NN):
    return lax.dot_general(a, b, dims, preferred_element_type=F32)


def halves(x):
    high = x.astype(BF)
    return high, (x - high.astype(F32)).astype(BF)


def dot_wide(a, b, dims=NN):
    ah, al = halves(a)
    bh, bl = halves(b)
    return dot(ah, bh, dims) + (dot(ah, bl, dims) + dot(al, bh, dims))


def dot_left(a, b, dims=NN):
    ah, al = halves(a)
    return dot(ah, b, dims) + dot(al, b, dims)


def sent_to_all(x, axis):
    copies = jnp.broadcast_to(x, (lax.axis_size(axis), *x.shape))
    return lax.all_to_all(copies, axis, split_axis=0, concat_axis=0, tiled=True)


def ring_gather(x, axis):
    n = lax.axis_size(axis)
    pieces = [x]
    for shift in (1, -1, -2):
        pieces.append(lax.ppermute(x, axis, [(i, (i + shift) % n) for i in range(n)]))
    return pieces


def places(index, n):
    return [index, lax.rem(index + n - 1, n), lax.rem(index + 1, n), lax.rem(index + 2, n)]


def fetches(core, across, near, mine_ref, other_ref, lanes, whole_ref, sems):
    copies = []
    for i, x in enumerate(across):
        for j, n in enumerate(near):
            for side, from_ref in enumerate((mine_ref, other_ref)):
                to = core if side == 0 else 1 - core
                copies.append(
                    pltpu.make_async_copy(
                        from_ref.at[i, j, :, :, lanes],
                        whole_ref.at[:, n, x, to],
                        sems.at[len(copies)],
                    )
                )
    return copies


def started(copies):
    for copy in copies:
        copy.start()


def finished(copies):
    for copy in copies:
        copy.wait()


def fade_rows(faded):
    high = faded.astype(BF).astype(F32)
    row = lax.broadcasted_iota(jnp.int32, (8, faded.shape[1]), 0)
    return jnp.where(row == 0, high, jnp.where(row == 1, faded - high, 0.0))


def fade_of(block):
    rows = block.shape[0]
    return block[rows - 8 : rows - 7] + block[rows - 7 : rows - 6]


def state_kernel(
    info_ref,
    own_ref,
    before_ref,
    after_ref,
    far_ref,
    gain_ref,
    mine_ref,
    other_ref,
    gap_ref,
    shift_ref,
    normed_out_ref,
    values_ref,
    opened_ref,
    cum_ref,
    growth_ref,
    payload_ref,
    whole_ref,
    sems,
    both_ref,
    tokens_ref,
    normed_ref,
    token_sems,
):
    rows, _ = normed_ref.shape
    cols = gap_ref.shape[1]
    block = own_ref.shape[0]
    spots = places(info_ref[1], rows // block)
    token_copies = [
        pltpu.make_async_copy(from_ref, tokens_ref.at[k], token_sems.at[k])
        for k, from_ref in enumerate((own_ref, before_ref, after_ref, far_ref))
    ]
    started(token_copies)
    copies = fetches(
        info_ref[0],
        range(mine_ref.shape[0]),
        range(mine_ref.shape[1]),
        mine_ref,
        other_ref,
        slice(None),
        whole_ref,
        sems,
    )
    started(copies)
    for k, spot in enumerate(spots):
        token_copies[k].wait()

        for i in range(block // 32):
            floats = tokens_ref[k, i * 32 : (i + 1) * 32, :].astype(F32)
            scale = lax.rsqrt(jnp.mean(floats * floats, axis=-1, keepdims=True) + EPSILON)
            at = pl.ds(pl.multiple_of(spot * block + i * 32, 32), 32)
            normed_ref[at, :] = (floats * scale * gain_ref[...]).astype(BF)
    handing = pltpu.make_async_copy(normed_ref, normed_out_ref, token_sems.at[len(spots)])
    handing.start()
    finished(copies)
    both_ref[...] = dot(normed_ref[...], whole_ref[...].reshape(-1, 2 * cols))
    row = lax.broadcasted_iota(jnp.int32, (CHUNK, CHUNK), 0)
    col = lax.broadcasted_iota(jnp.int32, (CHUNK, CHUNK), 1)
    tril = (row >= col).astype(BF)
    plane, height, _ = payload_ref.shape
    slab = height - 8
    heads = cols // RDIM
    states = [jnp.zeros((RDIM, RDIM), F32) for _ in range(heads)]
    faded = jnp.zeros((1, cols), F32)
    for c in range(rows // CHUNK):
        at = slice(c * CHUNK, (c + 1) * CHUNK)
        pre = both_ref[at, :cols].astype(BF).astype(F32)
        values = both_ref[at, cols:].astype(BF)
        opened = gap_ref[...] / (1.0 + jnp.exp(pre))
        shift = jnp.concatenate(
            [jnp.broadcast_to(shift_ref[h : h + 1, at], (RDIM, CHUNK)).T for h in range(heads)],
            axis=1,
        )
        decay = jnp.log1p(-opened) + shift
        d0, d1 = halves(decay)
        d2 = (decay - d0.astype(F32) - d1.astype(F32)).astype(BF)
        cum = dot(tril, d0) + (dot(tril, d1) + dot(tril, d2))
        total = cum[CHUNK - 1 :, :]
        kept = jnp.exp(total)
        key = opened * jnp.exp(total - cum)
        values_ref[at, :] = values
        opened_ref[at, :] = opened
        cum_ref[at, :] = cum
        faded = faded + total
        for h in range(heads):
            lanes = slice(h * RDIM, (h + 1) * RDIM)
            growth = dot_left_t(values[:, lanes], key[:, lanes])
            growth_ref[c, :, lanes] = growth
            states[h] = states[h] * kept[:, lanes] + growth
    fades = fade_rows(faded)
    for h in range(heads):
        lanes = slice(h * RDIM, (h + 1) * RDIM)
        for d in range(plane):
            block_d = jnp.concatenate(
                [states[h][d * slab : (d + 1) * slab], fades[:, lanes]], axis=0
            )
            payload_ref[d, :, lanes] = block_d.astype(BF)
    handing.wait()


def dot_left_t(values, key):
    kh, kl = halves(key)
    return dot(values, kh, TN) + dot(values, kl, TN)


def plane_kernel(got_ref, before_ref, faded_ref, total_ref):
    _, rows, cols = before_ref.shape
    state = jnp.zeros((rows, cols), F32)
    faded = jnp.zeros((1, cols), F32)
    for d in range(got_ref.shape[0]):
        got = got_ref[d].astype(F32)
        fade = fade_of(got)
        before_ref[d] = state
        faded_ref[d : d + 1, :] = faded
        state = state * jnp.exp(fade) + got[:rows]
        faded = faded + fade
    total = jnp.concatenate([state, fade_rows(faded)], axis=0).astype(BF)
    for z in range(total_ref.shape[0]):
        total_ref[z] = total


def depth_kernel(info_ref, totals_ref, before_ref, faded_ref, start_ref):
    near, far = totals_ref.shape[:2]
    devices, rows, cols = before_ref.shape
    state = jnp.zeros((rows, cols), F32)
    for z in range(far * near):
        got = totals_ref[z % near, z // near].astype(F32)
        new = state * jnp.exp(fade_of(got)) + got[:rows]
        state = jnp.where(z < info_ref[4], new, state)
    for d in range(devices):
        start_ref[d] = (before_ref[d] + jnp.exp(faded_ref[d : d + 1, :]) * state).astype(BF)


def inner_kernel(
    info_ref,
    normed_ref,
    mine_ref,
    other_ref,
    values_ref,
    opened_ref,
    cum_ref,
    pooled_ref,
    edge_ref,
    decayed_ref,
    heard_ref,
    whole_ref,
    sems,
    both_ref,
    held_ref,
    held_sem,
):
    rows, cols = values_ref.shape
    bringing = pltpu.make_async_copy(normed_ref, held_ref, held_sem.at[0])
    bringing.start()
    copies = fetches(
        info_ref[0],
        places(info_ref[3], mine_ref.shape[0]),
        places(info_ref[5], mine_ref.shape[1]),
        mine_ref,
        other_ref,
        slice(0, 2 * cols),
        whole_ref,
        sems,
    )
    started(copies)
    finished(copies)
    bringing.wait()
    both_ref[...] = dot(held_ref[...], whole_ref[...].reshape(-1, 2 * cols))
    pooled_ref[...] = both_ref[:, cols:].astype(BF)
    edge_ref[...] = both_ref[rows - RIM :, cols:].astype(BF)
    row = lax.broadcasted_iota(jnp.int32, (CHUNK, CHUNK), 0)
    col = lax.broadcasted_iota(jnp.int32, (CHUNK, CHUNK), 1)
    for h in range(cols // RDIM):
        lanes = slice(h * RDIM, (h + 1) * RDIM)
        for c in range(rows // CHUNK):
            at = slice(c * CHUNK, (c + 1) * CHUNK)
            cum = cum_ref[at, lanes]
            query = both_ref[at, lanes].astype(BF).astype(F32) * jnp.exp(cum)
            key = opened_ref[at, lanes] * jnp.exp(-cum)
            scores = jnp.where(row >= col, dot_wide(query, key, NT), 0.0)
            decayed_ref[at, lanes] = query
            heard_ref[at, lanes] = dot_left(scores, values_ref[at, lanes])


def pool_kernel(info_ref, pooled_ref, rim_ref, pool_ref):
    rows, cols = pool_ref.shape
    group = info_ref[1]
    padded = jnp.concatenate([rim_ref[...], pooled_ref[...]], axis=0).astype(F32)
    running = padded
    chosen = None
    for level in range(GROUPS):
        running = running + pltpu.roll(running, 2**level, 0)
        chosen = running if chosen is None else jnp.where(group == level, running, chosen)
    width = jnp.left_shift(jnp.int32(2), group)
    position = info_ref[2] + lax.broadcasted_iota(jnp.int32, (rows, cols), 0)
    divisor = jnp.minimum(position + 1, width).astype(F32)
    pool_ref[...] = (chosen[RIM:] / divisor - padded[RIM:]).astype(BF)


def final_kernel(
    info_ref,
    start_ref,
    growth_ref,
    cum_ref,
    decayed_ref,
    heard_ref,
    pool_ref,
    gain_ref,
    mine_ref,
    other_ref,
    part_ref,
    whole_ref,
    sems,
    mixed_ref,
    held_ref,
    out_sems,
):
    rows, cols = cum_ref.shape
    copies = fetches(
        info_ref[0],
        places(info_ref[3], mine_ref.shape[0]),
        places(info_ref[5], mine_ref.shape[1]),
        mine_ref,
        other_ref,
        slice(2 * cols, 4 * cols),
        whole_ref,
        sems,
    )
    started(copies)
    mixed_ref[:, :cols] = pool_ref[...]
    for h in range(cols // RDIM):
        lanes = slice(h * RDIM, (h + 1) * RDIM)
        state = start_ref[:, lanes].astype(F32)
        for c in range(rows // CHUNK):
            at = slice(c * CHUNK, (c + 1) * CHUNK)
            heard = heard_ref[at, lanes] + dot_wide(decayed_ref[at, lanes], state, NT)
            spread = lax.rsqrt(jnp.mean(heard * heard, axis=-1, keepdims=True) + EPSILON)
            mixed_ref[at, cols + h * RDIM : cols + (h + 1) * RDIM] = (
                heard * spread * gain_ref[...]
            ).astype(BF)
            total = cum_ref[(c + 1) * CHUNK - 1 : (c + 1) * CHUNK, lanes]
            state = state * jnp.exp(total) + growth_ref[c, :, lanes]

    finished(copies)
    far = whole_ref.shape[0]
    step = part_ref.shape[1] // far
    leaving = []
    for f in range(far):
        weight = whole_ref[f].reshape(step, 2 * cols)
        held_ref[f] = dot(mixed_ref[...], weight, NT).astype(BF)
        leaving.append(
            pltpu.make_async_copy(
                held_ref.at[f], part_ref.at[:, pl.ds(f * step, step)], out_sems.at[f]
            )
        )
        leaving[-1].start()
    finished(leaving)


VMEM = pl.BlockSpec(memory_space=pltpu.VMEM)
SMEM = pl.BlockSpec(memory_space=pltpu.SMEM)
HBM = pl.BlockSpec(memory_space=pltpu.HBM)


def spec_of(a):
    if a.dtype == jnp.int32:
        return SMEM
    return HBM if a.size * a.dtype.itemsize >= 1 << 19 and a.dtype == BF else VMEM


def call(kernel, outs, scratch, flops, moved, *args, out_specs=None):
    return pl.pallas_call(
        kernel,
        out_shape=outs,
        in_specs=[spec_of(a) for a in args],
        out_specs=out_specs or jax.tree.map(lambda _: VMEM, outs),
        scratch_shapes=scratch,
        cost_estimate=pl.CostEstimate(flops=flops, bytes_accessed=moved, transcendentals=0),
    )(*args)


def shape(dims, dtype):
    return jax.ShapeDtypeStruct(dims, dtype)


def side_by_side(*arrays):
    width = sum(a.shape[1] for a in arrays)
    total, at = None, 0
    for a in arrays:
        padded = jnp.pad(a, ((0, 0), (at, width - at - a.shape[1])))
        total = padded if total is None else total + padded
        at += a.shape[1]
    return total


def over_cores(x):
    return lax.ppermute(x, CORE, [(0, 1), (1, 0)])


def layer(
    tokens,
    norm_gain,
    pool_in_weight,
    query_weight,
    forget_weight,
    input_weight,
    forget_gap,
    decay_shift,
    out_gain,
    pool_out_weight,
    recur_out_weight,
):
    width = tokens.shape[1]
    cols = query_weight.shape[1]
    tp = lax.axis_size("tp")
    rows = tokens.shape[0] * tp
    devices = lax.axis_size(SP)
    info = jnp.stack(
        [
            lax.axis_index(CORE),
            lax.axis_index("tp"),
            lax.axis_index(SP) * rows,
            lax.axis_index(ACROSS),
            lax.axis_index(DEPTH),
            lax.axis_index(NEAR),
        ]
    ).astype(jnp.int32)

    pieces = ring_gather(tokens, "tp")
    weights = side_by_side(
        forget_weight,
        input_weight,
        query_weight,
        pool_in_weight,
        pool_out_weight.T,
        recur_out_weight.T,
    )
    weights = sent_to_all(weights, FAR)
    first = sent_to_all(weights[..., : 2 * cols], NEAR)
    first = sent_to_all(first, ACROSS)
    first_other = over_cores(first)
    rest = jnp.stack(ring_gather(weights[..., 2 * cols :], DEPTH))
    rest = jnp.stack(ring_gather(rest, ACROSS))
    rest_other = over_cores(rest)
    blocks = first.shape[2], first.shape[1], first.shape[0], 2, first.shape[3], 2 * cols
    whole = [
        pltpu.VMEM(blocks, BF),
        pltpu.SemaphoreType.DMA((2 * first.shape[0] * first.shape[1],)),
    ]

    plane = lax.axis_size(PLANE)
    slab = RDIM // plane
    normed, values, opened, cum, growth, payload = call(
        state_kernel,
        [
            shape((rows, width), BF),
            shape((rows, cols), BF),
            shape((rows, cols), F32),
            shape((rows, cols), F32),
            shape((rows // CHUNK, RDIM, cols), F32),
            shape((plane, slab + 8, cols), BF),
        ],
        [
            *whole,
            pltpu.VMEM((rows, 2 * cols), F32),
            pltpu.VMEM((tp, rows // tp, width), BF),
            pltpu.VMEM((rows, width), BF),
            pltpu.SemaphoreType.DMA((tp + 1,)),
        ],
        4 * rows * width * cols,
        8 << 20,
        info,
        *pieces,
        norm_gain[None, :],
        first,
        first_other,
        forget_gap[None, :],
        decay_shift,
        out_specs=[HBM, VMEM, VMEM, VMEM, VMEM, VMEM],
    )
    got = lax.all_to_all(payload, PLANE, split_axis=0, concat_axis=0, tiled=True)
    before, faded, total = call(
        plane_kernel,
        [
            shape((plane, slab, cols), F32),
            shape((plane, cols), F32),
            shape((lax.axis_size(FAR), slab + 8, cols), BF),
        ],
        [],
        1 << 20,
        1 << 19,
        got,
    )
    totals = lax.all_to_all(total, FAR, split_axis=0, concat_axis=0, tiled=True)
    totals = sent_to_all(totals, NEAR)
    start = call(
        depth_kernel,
        shape((plane, slab, cols), BF),
        [],
        1 << 20,
        1 << 19,
        info,
        totals,
        before,
        faded,
    )
    start = lax.all_to_all(
        start.reshape(RDIM, cols), PLANE, split_axis=0, concat_axis=0, tiled=True
    )
    pooled, edge, decayed, heard = call(
        inner_kernel,
        [
            shape((rows, cols), BF),
            shape((RIM, cols), BF),
            shape((rows, cols), F32),
            shape((rows, cols), F32),
        ],
        [
            *whole,
            pltpu.VMEM((rows, 2 * cols), F32),
            pltpu.VMEM((rows, width), BF),
            pltpu.SemaphoreType.DMA((1,)),
        ],
        4 * rows * width * cols,
        8 << 20,
        info,
        normed,
        rest,
        rest_other,
        values,
        opened,
        cum,
    )
    order = [(i - 1, i) for i in range(1, devices)]
    rim = lax.ppermute(edge, SP, order)
    pool = call(pool_kernel, shape((rows, cols), BF), [], 1 << 20, 1 << 19, info, pooled, rim)
    part = call(
        final_kernel,
        shape((rows, width), BF),
        [
            *whole,
            pltpu.VMEM((rows, 2 * cols), BF),
            pltpu.VMEM((blocks[0], rows, width // blocks[0]), BF),
            pltpu.SemaphoreType.DMA((blocks[0],)),
        ],
        4 * rows * width * cols,
        8 << 20,
        info,
        start,
        growth,
        cum,
        decayed,
        heard,
        pool,
        out_gain[None, :],
        rest,
        rest_other,
        out_specs=HBM,
    )
    parts = lax.all_to_all(
        part.reshape(tp, rows // tp, width), "tp", split_axis=0, concat_axis=0, tiled=True
    )
    return jnp.sum(parts.astype(F32), axis=0).astype(BF)


def solution(mesh):
    split = Mesh(mesh.devices.reshape(4, 4, 4, 2, mesh.shape["tp"]), SP_TP)
    in_specs = (
        P(SP_TP, None),
        P(),
        P(SP, "tp"),
        P(SP, "tp"),
        P(SP, "tp"),
        P(SP, "tp"),
        P("tp"),
        P("tp", SP),
        P(),
        P("tp", SP),
        P("tp", SP),
    )
    out_specs = P(SP_TP, None)
    return jax.shard_map(layer, mesh=split, in_specs=in_specs, out_specs=out_specs, check_vma=False)
```

profile of v0, /device:TPU:6, one launch (start us, length us, event | category | flops | bytes accessed | tf_op | source)
XLA Modules:
  0.0 229.7 jit_solution(15957401163522295960)
XLA Ops:
  0.0 0.8 pad_add_fusion
  0.8 31.8 %all_to_all.43 = bf16[4,16,1536]{2,1,0:T(8,128)(2,1)S(1)} all-to-all(bf16[4,16,1536]{2,1,0:T(8,128)(2,1)S(1)} %broadcast_in_dim.22), channel_id=1, replica_groups=mesh['sp_f'=4,'sp_n'=4,'sp_x'=4,'sp_c'=2,'tp'=4] {'sp_f'}, dimensions={0} | all-to-all | bytes 393216 | tf_op jit(solution)/shard_map/all_to_all | solution.py:49
  32.6 0.7 broadcast_in_dim.23
  33.4 4.6 %all-to-all-start.1 = ((bf16[4,4,16,512]{3,2,1,0:T(8,128)(2,1)}), bf16[4,4,16,512]{3,2,1,0:T(8,128)(2,1)S(1)}, u32[]{:S(2)}, u32[]{:S(2)}) async-start(bf16[4,4,16,512]{3,2,1,0:T(8,128)(2,1)} %broadcast_in_dim.23), calls=%async_computation.1 | async-start | bytes 524288 | tf_op jit(solution)/shard_map/all_to_all | solution.py:49
  38.0 4.2 %collective-permute-start.6 = (bf16[4,16,1024]{2,1,0:T(8,128)(2,1)S(1)}, bf16[4,16,1024]{2,1,0:T(8,128)(2,1)S(1)}, u32[]{:S(2)}, u32[]{:S(2)}) collective-permute-start(bf16[4,16,1024]{2,1,0:T(8,128)(2,1)S(1)} %get-tuple-element.34), channel_id=1, source_target_pairs={{0,448},{32,480},{64,0},{96,32},{128,64},{160,96},{192,128},{224,1... | collective-permute-start | bytes 393224 | tf_op jit(solution)/shard_map/ppermute | solution.py:56
  42.2 2.5 %collective-permute-start.5 = (bf16[4,16,1024]{2,1,0:T(8,128)(2,1)S(1)}, bf16[4,16,1024]{2,1,0:T(8,128)(2,1)S(1)}, u32[]{:S(2)}, u32[]{:S(2)}) collective-permute-start(bf16[4,16,1024]{2,1,0:T(8,128)(2,1)S(1)} %get-tuple-element.34), channel_id=1, source_target_pairs={{0,480},{32,0},{64,32},{96,64},{128,96},{160,128},{192,160},{224,1... | collective-permute-start | bytes 393224 | tf_op jit(solution)/shard_map/ppermute | solution.py:56
  44.6 3.4 %collective-permute-start.4 = (bf16[4,16,1024]{2,1,0:T(8,128)(2,1)S(1)}, bf16[4,16,1024]{2,1,0:T(8,128)(2,1)S(1)}, u32[]{:S(2)}, u32[]{:S(2)}) collective-permute-start(bf16[4,16,1024]{2,1,0:T(8,128)(2,1)S(1)} %get-tuple-element.34), channel_id=1, source_target_pairs={{0,32},{32,64},{64,96},{96,128},{128,160},{160,192},{192,224},{224... | collective-permute-start | bytes 393224 | tf_op jit(solution)/shard_map/ppermute | solution.py:56
  48.0 4.2 %collective-permute-done.6 = bf16[4,16,1024]{2,1,0:T(8,128)(2,1)S(1)} collective-permute-done((bf16[4,16,1024]{2,1,0:T(8,128)(2,1)S(1)}, bf16[4,16,1024]{2,1,0:T(8,128)(2,1)S(1)}, u32[]{:S(2)}, u32[]{:S(2)}) %collective-permute-start.6) | collective-permute-done | bytes 131104 | tf_op jit(solution)/shard_map/ppermute | solution.py:56
  52.2 0.0 collective-permute-done.5
  52.2 0.5 collective-permute-done.4
  52.7 0.9 fusion
  53.6 3.3 %collective-permute-start.9 = (bf16[4,4,16,1024]{3,2,1,0:T(8,128)(2,1)S(1)}, bf16[4,4,16,1024]{3,2,1,0:T(8,128)(2,1)S(1)}, u32[]{:S(2)}, u32[]{:S(2)}) collective-permute-start(bf16[4,4,16,1024]{3,2,1,0:T(8,128)(2,1)S(1)} %get-tuple-element.32), channel_id=1, source_target_pairs={{0,16},{8,24},{16,0},{24,8},{1,17},{9,25},{17,1},{25,9},{2,18},{10... | collective-permute-start | bytes 1572872 | tf_op jit(solution)/shard_map/ppermute | solution.py:56
  56.9 1.9 collective-permute-start.8
  58.8 5.1 %collective-permute-start.7 = (bf16[4,4,16,1024]{3,2,1,0:T(8,128)(2,1)S(1)}, bf16[4,4,16,1024]{3,2,1,0:T(8,128)(2,1)}, u32[]{:S(2)}, u32[]{:S(2)}) collective-permute-start(bf16[4,4,16,1024]{3,2,1,0:T(8,128)(2,1)S(1)} %get-tuple-element.32), channel_id=1, source_target_pairs={{0,8},{8,16},{16,24},{24,0},{1,9},{9,17},{17,25},{25,1},{2,10},{10... | collective-permute-start | bytes 1572872 | tf_op jit(solution)/shard_map/ppermute | solution.py:56
  64.0 0.0 all-to-all-done.1
  64.0 1.1 broadcast_in_dim.24
  65.1 4.5 %all-to-all-start.2 = ((bf16[4,4,4,16,512]{4,3,2,1,0:T(8,128)(2,1)}), bf16[4,4,4,16,512]{4,3,2,1,0:T(8,128)(2,1)S(1)}, u32[]{:S(2)}, u32[]{:S(2)}) async-start(bf16[4,4,4,16,512]{4,3,2,1,0:T(8,128)(2,1)} %broadcast_in_dim.24), calls=%async_computation.2 | async-start | bytes 2097152 | tf_op jit(solution)/shard_map/all_to_all | solution.py:49
  69.6 2.2 collective-permute-done.9
  71.8 0.0 copy-start.2
  71.8 8.7 %collective-permute-done.8 = bf16[4,4,16,1024]{3,2,1,0:T(8,128)(2,1)S(1)} collective-permute-done((bf16[4,4,16,1024]{3,2,1,0:T(8,128)(2,1)S(1)}, bf16[4,4,16,1024]{3,2,1,0:T(8,128)(2,1)S(1)}, u32[]{:S(2)}, u32[]{:S(2)}) %collective-permute-start.8) | collective-permute-done | bytes 524320 | tf_op jit(solution)/shard_map/ppermute | solution.py:56
  80.5 0.0 copy-start.3
  80.5 0.4 collective-permute-done.7
  80.9 0.0 copy-done.2
  80.9 0.4 copy-done.3
  81.3 1.8 pad_maximum_fusion.mine_ref
  83.1 0.0 copy-start
  83.1 1.9 collective-permute-start.10
  85.0 5.5 %all-to-all-done.2.mine_ref = bf16[4,4,4,16,512]{4,3,2,1,0:T(8,128)(2,1)S(1)} async-done(((bf16[4,4,4,16,512]{4,3,2,1,0:T(8,128)(2,1)}), bf16[4,4,4,16,512]{4,3,2,1,0:T(8,128)(2,1)S(1)}, u32[]{:S(2)}, u32[]{:S(2)}) %all-to-all-start.2) | async-done | bytes 1048608 | tf_op jit(solution)/shard_map/all_to_all | solution.py:49
  90.5 0.0 copy-start.1
  90.5 1.9 collective-permute-start.3
  92.5 3.5 %collective-permute-start = (bf16[128,2048]{1,0:T(8,128)(2,1)}, bf16[128,2048]{1,0:T(8,128)(2,1)}, u32[]{:S(2)}, u32[]{:S(2)}) collective-permute-start(bf16[128,2048]{1,0:T(8,128)(2,1)} %own_ref.1), channel_id=1, source_target_pairs={{0,1},{1,2},{2,3},{3,0},{4,5},{5,6},{6,7},{7,4},{8,9},{9,10},{10,1... | collective-permute-start | bytes 1572872 | tf_op jit(solution)/shard_map/ppermute | solution.py:56
  96.0 3.6 %collective-permute-start.1 = (bf16[128,2048]{1,0:T(8,128)(2,1)}, bf16[128,2048]{1,0:T(8,128)(2,1)}, u32[]{:S(2)}, u32[]{:S(2)}) collective-permute-start(bf16[128,2048]{1,0:T(8,128)(2,1)} %own_ref.1), channel_id=1, source_target_pairs={{0,3},{1,0},{2,1},{3,2},{4,7},{5,4},{6,5},{7,6},{8,11},{9,8},{10,9... | collective-permute-start | bytes 1572872 | tf_op jit(solution)/shard_map/ppermute | solution.py:56
  99.5 3.9 %collective-permute-start.2 = (bf16[128,2048]{1,0:T(8,128)(2,1)}, bf16[128,2048]{1,0:T(8,128)(2,1)}, u32[]{:S(2)}, u32[]{:S(2)}) collective-permute-start(bf16[128,2048]{1,0:T(8,128)(2,1)} %own_ref.1), channel_id=1, source_target_pairs={{0,2},{1,3},{2,0},{3,1},{4,6},{5,7},{6,4},{7,5},{8,10},{9,11},{10,... | collective-permute-start | bytes 1572872 | tf_op jit(solution)/shard_map/ppermute | solution.py:56
  103.5 0.6 stack.57.info_ref
  104.1 6.2 %collective-permute-done.before_ref = bf16[128,2048]{1,0:T(8,128)(2,1)} collective-permute-done((bf16[128,2048]{1,0:T(8,128)(2,1)}, bf16[128,2048]{1,0:T(8,128)(2,1)}, u32[]{:S(2)}, u32[]{:S(2)}) %collective-permute-start) | collective-permute-done | bytes 524320 | tf_op jit(solution)/shard_map/ppermute | solution.py:56
  110.3 2.7 %collective-permute-done.1.after_ref = bf16[128,2048]{1,0:T(8,128)(2,1)} collective-permute-done((bf16[128,2048]{1,0:T(8,128)(2,1)}, bf16[128,2048]{1,0:T(8,128)(2,1)}, u32[]{:S(2)}, u32[]{:S(2)}) %collective-permute-start.1) | collective-permute-done | bytes 524320 | tf_op jit(solution)/shard_map/ppermute | solution.py:56
  113.0 9.7 %collective-permute-done.2.far_ref = bf16[128,2048]{1,0:T(8,128)(2,1)} collective-permute-done((bf16[128,2048]{1,0:T(8,128)(2,1)}, bf16[128,2048]{1,0:T(8,128)(2,1)}, u32[]{:S(2)}, u32[]{:S(2)}) %collective-permute-start.2) | collective-permute-done | bytes 524320 | tf_op jit(solution)/shard_map/ppermute | solution.py:56
  122.7 0.0 collective-permute-done.3.other_ref
  122.7 0.0 copy-done.1
  122.7 7.7 %shard_map.109 = (bf16[512,2048]{1,0:T(8,128)(2,1)}, bf16[512,256]{1,0:T(8,128)(2,1)}, f32[512,256]{1,0:T(8,128)}, f32[512,256]{1,0:T(8,128)}, f32[4,128,256]{2,1,0:T(8,128)}, /*index=5*/bf16[8,24,256]{2,1,0:T(8,128)(2,1)}) custom-call(s32[6]{0:T(128)} %stack.57.info_ref, bf16[128,2048]{1,0:T(8,128)(2,1)} %own_ref.1, ...), custom_call_target="tpu_custom_call" | custom-call | flops 1073741824 | bytes 8388608 | tf_op jit(solution)/shard_map/pallas_call | solution.py:372
  130.4 0.0 copy-done
  130.4 8.6 %all_to_all.44.got_ref = bf16[8,24,256]{2,1,0:T(8,128)(2,1)} all-to-all(bf16[8,24,256]{2,1,0:T(8,128)(2,1)} %get-tuple-element.18), channel_id=1, replica_groups=mesh['sp_f'=4,'sp_n'=4,'sp_x'=4,'sp_c'=2,'tp'=4] {'sp_x','sp_c'}, dimensions={0} | all-to-all | bytes 196608 | tf_op jit(solution)/shard_map/all_to_all | solution.py:481
  139.1 1.6 shard_map.110
  140.7 19.2 %all_to_all.45 = bf16[4,24,256]{2,1,0:T(8,128)(2,1)S(1)} all-to-all(bf16[4,24,256]{2,1,0:T(8,128)(2,1)} %get-tuple-element.19), channel_id=1, replica_groups=mesh['sp_f'=4,'sp_n'=4,'sp_x'=4,'sp_c'=2,'tp'=4] {'sp_f'}, dimensions={0} | all-to-all | bytes 98304 | tf_op jit(solution)/shard_map/all_to_all | solution.py:494
  159.9 9.9 %all_to_all.46.totals_ref = bf16[4,4,24,256]{3,2,1,0:T(8,128)(2,1)} all-to-all(bf16[4,4,24,256]{3,2,1,0:T(8,128)(2,1)S(1)} %broadcast_in_dim.26), channel_id=1, replica_groups=mesh['sp_f'=4,'sp_n'=4,'sp_x'=4,'sp_c'=2,'tp'=4] {'sp_n'}, dimensions={0} | all-to-all | bytes 393216 | tf_op jit(solution)/shard_map/all_to_all | solution.py:49
  169.8 1.7 shard_map.111
  171.5 5.4 %all-to-all-start.6 = ((bf16[8,16,256]{2,1,0:T(8,128)(2,1)}), bf16[8,16,256]{2,1,0:T(8,128)(2,1)S(1)}, u32[]{:S(2)}, u32[]{:S(2)}) async-start(bf16[8,16,256]{2,1,0:T(8,128)(2,1)} %shard_map.111), calls=%async_computation.6 | async-start | bytes 131072 | tf_op jit(solution)/shard_map/all_to_all | solution.py:507
  176.9 0.0 collective-permute-done.10.other_ref
  176.9 7.7 %shard_map.112 = (bf16[512,256]{1,0:T(8,128)(2,1)}, bf16[16,256]{1,0:T(8,128)(2,1)}, f32[512,256]{1,0:T(8,128)}, f32[512,256]{1,0:T(8,128)}) custom-call(s32[6]{0:T(128)} %stack.57.info_ref, bf16[512,2048]{1,0:T(8,128)(2,1)} %get-tuple-element.24.normed_ref, bf16[4,4,4,16,1024]{4,3,2,1,0:T(8,128)(2,1)} %copy-done, ...), custom_call_target="tpu_custom_call" | custom-call | flops 1073741824 | bytes 8388608 | tf_op jit(solution)/shard_map/pallas_call | solution.py:372
  184.5 2.0 collective-permute-start.11
  186.6 3.1 %collective-permute-done.11.rim_ref = bf16[16,256]{1,0:T(8,128)(2,1)S(1)} collective-permute-done((bf16[16,256]{1,0:T(8,128)(2,1)}, bf16[16,256]{1,0:T(8,128)(2,1)S(1)}, u32[]{:S(2)}, u32[]{:S(2)}) %collective-permute-start.11) | collective-permute-done | bytes 8224 | tf_op jit(solution)/shard_map/ppermute | solution.py:535
  189.7 0.0 copy-start.5
  189.7 0.6 copy-done.5
  190.3 2.0 shard_map.113.pool_ref
  192.3 0.0 all-to-all-done.6
  192.3 0.0 copy-start.4
  192.3 0.6 copy-done.4
  193.0 5.7 %shard_map.114 = bf16[512,2048]{1,0:T(8,128)(2,1)} custom-call(s32[6]{0:T(128)} %stack.57.info_ref, bf16[128,256]{1,0:T(8,128)(2,1)} %bitcast.26, f32[4,128,256]{2,1,0:T(8,128)} %get-tuple-element.22.growth_ref, f32[512,256]{1,0:T(8,128)} %get-tuple-element.23.cum_ref, f32[512,256]{1,0:T(8,128)} %get-tuple-element.27.decayed_ref, ...), custom_call_target="tpu_custom_call" | custom-call | flops 1073741824 | bytes 8388608 | tf_op jit(solution)/shard_map/pallas_call | solution.py:372
  198.6 29.8 %all_to_all.47 = bf16[4,128,2048]{2,1,0:T(8,128)(2,1)S(1)} all-to-all(bf16[4,128,2048]{2,1,0:T(8,128)(2,1)} %bitcast.23), channel_id=1, replica_groups=mesh['sp_f'=4,'sp_n'=4,'sp_x'=4,'sp_c'=2,'tp'=4] {'tp'}, dimensions={0} | all-to-all | bytes 4194304 | tf_op jit(solution)/shard_map/all_to_all | solution.py:560
  228.4 1.3 reduce_sum.12
  (4 shorter events, 0.1 us)
Async XLA Ops:
  33.4 30.6 %all-to-all-start.1 = ((bf16[4,4,16,512]{3,2,1,0:T(8,128)(2,1)}), bf16[4,4,16,512]{3,2,1,0:T(8,128)(2,1)S(1)}, u32[]{:S(2)}, u32[]{:S(2)}) async-start(bf16[4,4,16,512]{3,2,1,0:T(8,128)(2,1)} %broadcast_in_dim.23), calls=%async_computation.1 | async-start | bytes 524288 | tf_op jit(solution)/shard_map/all_to_all | solution.py:49
  38.0 14.2 %collective-permute-start.6 = (bf16[4,16,1024]{2,1,0:T(8,128)(2,1)S(1)}, bf16[4,16,1024]{2,1,0:T(8,128)(2,1)S(1)}, u32[]{:S(2)}, u32[]{:S(2)}) collective-permute-start(bf16[4,16,1024]{2,1,0:T(8,128)(2,1)S(1)} %get-tuple-element.34), channel_id=1, source_target_pairs={{0,448},{32,480},{64,0},{96,32},{128,64},{160,96},{192,128},{224,1... | collective-permute-start | bytes 393224 | tf_op jit(solution)/shard_map/ppermute | solution.py:56
  42.2 10.1 %collective-permute-start.5 = (bf16[4,16,1024]{2,1,0:T(8,128)(2,1)S(1)}, bf16[4,16,1024]{2,1,0:T(8,128)(2,1)S(1)}, u32[]{:S(2)}, u32[]{:S(2)}) collective-permute-start(bf16[4,16,1024]{2,1,0:T(8,128)(2,1)S(1)} %get-tuple-element.34), channel_id=1, source_target_pairs={{0,480},{32,0},{64,32},{96,64},{128,96},{160,128},{192,160},{224,1... | collective-permute-start | bytes 393224 | tf_op jit(solution)/shard_map/ppermute | solution.py:56
  44.6 8.1 %collective-permute-start.4 = (bf16[4,16,1024]{2,1,0:T(8,128)(2,1)S(1)}, bf16[4,16,1024]{2,1,0:T(8,128)(2,1)S(1)}, u32[]{:S(2)}, u32[]{:S(2)}) collective-permute-start(bf16[4,16,1024]{2,1,0:T(8,128)(2,1)S(1)} %get-tuple-element.34), channel_id=1, source_target_pairs={{0,32},{32,64},{64,96},{96,128},{128,160},{160,192},{192,224},{224... | collective-permute-start | bytes 393224 | tf_op jit(solution)/shard_map/ppermute | solution.py:56
  53.6 18.2 %collective-permute-start.9 = (bf16[4,4,16,1024]{3,2,1,0:T(8,128)(2,1)S(1)}, bf16[4,4,16,1024]{3,2,1,0:T(8,128)(2,1)S(1)}, u32[]{:S(2)}, u32[]{:S(2)}) collective-permute-start(bf16[4,4,16,1024]{3,2,1,0:T(8,128)(2,1)S(1)} %get-tuple-element.32), channel_id=1, source_target_pairs={{0,16},{8,24},{16,0},{24,8},{1,17},{9,25},{17,1},{25,9},{2,18},{10... | collective-permute-start | bytes 1572872 | tf_op jit(solution)/shard_map/ppermute | solution.py:56
  56.9 23.6 %collective-permute-start.8 = (bf16[4,4,16,1024]{3,2,1,0:T(8,128)(2,1)S(1)}, bf16[4,4,16,1024]{3,2,1,0:T(8,128)(2,1)S(1)}, u32[]{:S(2)}, u32[]{:S(2)}) collective-permute-start(bf16[4,4,16,1024]{3,2,1,0:T(8,128)(2,1)S(1)} %get-tuple-element.32), channel_id=1, source_target_pairs={{0,24},{8,0},{16,8},{24,16},{1,25},{9,1},{17,9},{25,17},{2,26},{10... | collective-permute-start | bytes 1572872 | tf_op jit(solution)/shard_map/ppermute | solution.py:56
  58.8 22.1 %collective-permute-start.7 = (bf16[4,4,16,1024]{3,2,1,0:T(8,128)(2,1)S(1)}, bf16[4,4,16,1024]{3,2,1,0:T(8,128)(2,1)}, u32[]{:S(2)}, u32[]{:S(2)}) collective-permute-start(bf16[4,4,16,1024]{3,2,1,0:T(8,128)(2,1)S(1)} %get-tuple-element.32), channel_id=1, source_target_pairs={{0,8},{8,16},{16,24},{24,0},{1,9},{9,17},{17,25},{25,1},{2,10},{10... | collective-permute-start | bytes 1572872 | tf_op jit(solution)/shard_map/ppermute | solution.py:56
  65.1 25.4 %all-to-all-start.2 = ((bf16[4,4,4,16,512]{4,3,2,1,0:T(8,128)(2,1)}), bf16[4,4,4,16,512]{4,3,2,1,0:T(8,128)(2,1)S(1)}, u32[]{:S(2)}, u32[]{:S(2)}) async-start(bf16[4,4,4,16,512]{4,3,2,1,0:T(8,128)(2,1)} %broadcast_in_dim.24), calls=%async_computation.2 | async-start | bytes 2097152 | tf_op jit(solution)/shard_map/all_to_all | solution.py:49
  71.8 9.1 %copy-start.2 = (bf16[4,4,16,1024]{3,2,1,0:T(8,128)(2,1)}, bf16[4,4,16,1024]{3,2,1,0:T(8,128)(2,1)S(1)}, u32[]{:S(2)}) copy-start(bf16[4,4,16,1024]{3,2,1,0:T(8,128)(2,1)S(1)} %collective-permute-done.9) | copy-start | bytes 1572868
  80.5 0.8 copy-start.3
  83.1 47.3 %copy-start = (bf16[4,4,4,16,1024]{4,3,2,1,0:T(8,128)(2,1)}, bf16[4,4,4,16,1024]{4,3,2,1,0:T(8,128)(2,1)S(1)}, u32[]{:S(2)}) copy-start(bf16[4,4,4,16,1024]{4,3,2,1,0:T(8,128)(2,1)S(1)} %pad_maximum_fusion.mine_ref) | copy-start | bytes 6291460
  83.1 93.8 %collective-permute-start.10 = (bf16[4,4,4,16,1024]{4,3,2,1,0:T(8,128)(2,1)S(1)}, bf16[4,4,4,16,1024]{4,3,2,1,0:T(8,128)(2,1)}, u32[]{:S(2)}, u32[]{:S(2)}) collective-permute-start(bf16[4,4,4,16,1024]{4,3,2,1,0:T(8,128)(2,1)S(1)} %pad_maximum_fusion.mine_ref), channel_id=1, source_target_pairs={{0,4},{4,0},{1,5},{5,1},{2,6},{6,2},{3,7},{7,3},{8,12},{12,8},{9,1... | collective-permute-start | bytes 6291464 | tf_op jit(solution)/shard_map/ppermute | solution.py:397
  90.5 32.2 %copy-start.1 = (bf16[4,4,4,16,512]{4,3,2,1,0:T(8,128)(2,1)}, bf16[4,4,4,16,512]{4,3,2,1,0:T(8,128)(2,1)S(1)}, u32[]{:S(2)}) copy-start(bf16[4,4,4,16,512]{4,3,2,1,0:T(8,128)(2,1)S(1)} %all-to-all-done.2.mine_ref) | copy-start | bytes 3145732
  90.5 32.1 %collective-permute-start.3 = (bf16[4,4,4,16,512]{4,3,2,1,0:T(8,128)(2,1)S(1)}, bf16[4,4,4,16,512]{4,3,2,1,0:T(8,128)(2,1)}, u32[]{:S(2)}, u32[]{:S(2)}) collective-permute-start(bf16[4,4,4,16,512]{4,3,2,1,0:T(8,128)(2,1)S(1)} %all-to-all-done.2.mine_ref), channel_id=1, source_target_pairs={{0,4},{4,0},{1,5},{5,1},{2,6},{6,2},{3,7},{7,3},{8,12},{12,8},{9,1... | collective-permute-start | bytes 3145736 | tf_op jit(solution)/shard_map/ppermute | solution.py:397
  92.5 17.8 %collective-permute-start = (bf16[128,2048]{1,0:T(8,128)(2,1)}, bf16[128,2048]{1,0:T(8,128)(2,1)}, u32[]{:S(2)}, u32[]{:S(2)}) collective-permute-start(bf16[128,2048]{1,0:T(8,128)(2,1)} %own_ref.1), channel_id=1, source_target_pairs={{0,1},{1,2},{2,3},{3,0},{4,5},{5,6},{6,7},{7,4},{8,9},{9,10},{10,1... | collective-permute-start | bytes 1572872 | tf_op jit(solution)/shard_map/ppermute | solution.py:56
  96.0 17.0 %collective-permute-start.1 = (bf16[128,2048]{1,0:T(8,128)(2,1)}, bf16[128,2048]{1,0:T(8,128)(2,1)}, u32[]{:S(2)}, u32[]{:S(2)}) collective-permute-start(bf16[128,2048]{1,0:T(8,128)(2,1)} %own_ref.1), channel_id=1, source_target_pairs={{0,3},{1,0},{2,1},{3,2},{4,7},{5,4},{6,5},{7,6},{8,11},{9,8},{10,9... | collective-permute-start | bytes 1572872 | tf_op jit(solution)/shard_map/ppermute | solution.py:56
  99.5 23.2 %collective-permute-start.2 = (bf16[128,2048]{1,0:T(8,128)(2,1)}, bf16[128,2048]{1,0:T(8,128)(2,1)}, u32[]{:S(2)}, u32[]{:S(2)}) collective-permute-start(bf16[128,2048]{1,0:T(8,128)(2,1)} %own_ref.1), channel_id=1, source_target_pairs={{0,2},{1,3},{2,0},{3,1},{4,6},{5,7},{6,4},{7,5},{8,10},{9,11},{10,... | collective-permute-start | bytes 1572872 | tf_op jit(solution)/shard_map/ppermute | solution.py:56
  171.5 20.8 %all-to-all-start.6 = ((bf16[8,16,256]{2,1,0:T(8,128)(2,1)}), bf16[8,16,256]{2,1,0:T(8,128)(2,1)S(1)}, u32[]{:S(2)}, u32[]{:S(2)}) async-start(bf16[8,16,256]{2,1,0:T(8,128)(2,1)} %shard_map.111), calls=%async_computation.6 | async-start | bytes 131072 | tf_op jit(solution)/shard_map/all_to_all | solution.py:507
  184.5 5.2 %collective-permute-start.11 = (bf16[16,256]{1,0:T(8,128)(2,1)}, bf16[16,256]{1,0:T(8,128)(2,1)S(1)}, u32[]{:S(2)}, u32[]{:S(2)}) collective-permute-start(bf16[16,256]{1,0:T(8,128)(2,1)} %get-tuple-element.30), channel_id=1, source_target_pairs={{0,4},{4,8},{8,12},{12,16},{16,20},{20,24},{24,28},{28,32},{32,36}... | collective-permute-start | bytes 24584 | tf_op jit(solution)/shard_map/ppermute | solution.py:535
  189.7 0.6 copy-start.5
  192.3 0.6 copy-start.4
where the time goes:
time: 233 us; the launch traced here: 230 us
  blocking collectives  99.3 us (43%)
  starting transfers between devices  51.6 us (22%)
  waiting for transfers between devices  43.3 us (19%)
  Pallas kernels  26.4 us (11%)
  other arithmetic  4.75 us (2%)
  local copies, waits for them, and re-layouts  4.12 us (2%)
    all_to_all x2, blocking collectives, sent_to_all(): return lax.all_to_all(copies, axis, split_axis=0, concat_axis=0, tiled=True)  41.7 us
    ppermute x9, waiting for transfers between devices, ring_gather(): lax.ppermute(x, axis, [(i, (i + shift) % n) for i in range(n)])  34.6 us
    ppermute x9, starting transfers between devices, ring_gather(): lax.ppermute(x, axis, [(i, (i + shift) % n) for i in range(n)])  31.3 us
    all_to_all x1, blocking collectives, layer(): lax.all_to_all(part.reshape(tp, rows // tp, width), 'tp', split_axis=0, c...  29.8 us
    pallas_call x6, Pallas kernels, call(): pl.pallas_call(kernel, out_shape=outs, in_specs=[spec_of(a) for a in args...  26.4 us
    all_to_all x1, blocking collectives, layer(): totals = lax.all_to_all(total, FAR, split_axis=0, concat_axis=0, tiled=True)  19.2 us
    all_to_all x2, starting transfers between devices, sent_to_all(): return lax.all_to_all(copies, axis, split_axis=0, concat_axis=0, tiled=True)  9.12 us
    all_to_all x1, blocking collectives, layer(): lax.all_to_all(payload, PLANE, split_axis=0, concat_axis=0, tiled=True)  8.62 us
  transfers between devices with their start and end apart: 15, of which 10 were waited for; matrix products, arithmetic and copies ran while one was open for 2% of the time, Pallas kernels for 9%

commit v1 on v0

--- a/solution.py
+++ b/solution.py
@@ -220,11 +220,11 @@
 
 
 def depth_kernel(info_ref, totals_ref, before_ref, faded_ref, start_ref):
-    near, far = totals_ref.shape[:2]
+    planes = totals_ref.shape[0]
     devices, rows, cols = before_ref.shape
     state = jnp.zeros((rows, cols), F32)
-    for z in range(far * near):
-        got = totals_ref[z % near, z // near].astype(F32)
+    for z in range(planes):
+        got = totals_ref[z].astype(F32)
         new = state * jnp.exp(fade_of(got)) + got[:rows]
         state = jnp.where(z < info_ref[4], new, state)
     for d in range(devices):
@@ -484,15 +484,14 @@
         [
             shape((plane, slab, cols), F32),
             shape((plane, cols), F32),
-            shape((lax.axis_size(FAR), slab + 8, cols), BF),
+            shape((lax.axis_size(DEPTH), slab + 8, cols), BF),
         ],
         [],
         1 << 20,
         1 << 19,
         got,
     )
-    totals = lax.all_to_all(total, FAR, split_axis=0, concat_axis=0, tiled=True)
-    totals = sent_to_all(totals, NEAR)
+    totals = lax.all_to_all(total, DEPTH, split_axis=0, concat_axis=0, tiled=True)
     start = call(
         depth_kernel,
         shape((plane, slab, cols), BF),

time: 233 us -> 226 us (0.970)
  blocking collectives: 99.3 us -> 93.1 us
    all_to_all x2 -> x1, blocking collectives: 41.7 us -> 31.8 us  [sent_to_all(): return lax.all_to_all(copies, axis, split_axis=0, concat_axis=0, tiled=True)]
    all_to_all x1, blocking collectives: 19.2 us -> 22.8 us  [layer(): lax.all_to_all(total, DEPTH, split_axis=0, concat_axis=0, tiled=True)]
where the time goes in v1:
time: 226 us; the launch traced here: 224 us
  blocking collectives  93.1 us (41%)
  starting transfers between devices  51.6 us (23%)
  waiting for transfers between devices  43.3 us (19%)
  Pallas kernels  26.5 us (12%)
  other arithmetic  4.75 us (2%)
  local copies, waits for them, and re-layouts  4.11 us (2%)
    ppermute x9, waiting for transfers between devices, ring_gather(): lax.ppermute(x, axis, [(i, (i + shift) % n) for i in range(n)])  34.6 us
    all_to_all x1, blocking collectives, sent_to_all(): return lax.all_to_all(copies, axis, split_axis=0, concat_axis=0, tiled=True)  31.8 us
    ppermute x9, starting transfers between devices, ring_gather(): lax.ppermute(x, axis, [(i, (i + shift) % n) for i in range(n)])  31.3 us
    all_to_all x1, blocking collectives, layer(): lax.all_to_all(part.reshape(tp, rows // tp, width), 'tp', split_axis=0, c...  29.9 us
    pallas_call x6, Pallas kernels, call(): pl.pallas_call(kernel, out_shape=outs, in_specs=[spec_of(a) for a in args...  26.5 us
    all_to_all x1, blocking collectives, layer(): lax.all_to_all(total, DEPTH, split_axis=0, concat_axis=0, tiled=True)  22.8 us
    all_to_all x2, starting transfers between devices, sent_to_all(): return lax.all_to_all(copies, axis, split_axis=0, concat_axis=0, tiled=True)  9.12 us
    all_to_all x1, blocking collectives, layer(): lax.all_to_all(payload, PLANE, split_axis=0, concat_axis=0, tiled=True)  8.62 us
  transfers between devices with their start and end apart: 15, of which 10 were waited for; matrix products, arithmetic and copies ran while one was open for 2% of the time, Pallas kernels for 9%

profile of v1, /device:TPU:6, one launch (start us, length us, event | category | flops | bytes accessed | tf_op | source)
XLA Modules:
  0.0 223.6 jit_solution(18394925080006411215)
XLA Ops:
  0.0 0.8 pad_add_fusion
  0.8 31.8 %all_to_all.38 = bf16[4,16,1536]{2,1,0:T(8,128)(2,1)S(1)} all-to-all(bf16[4,16,1536]{2,1,0:T(8,128)(2,1)S(1)} %broadcast_in_dim.19), channel_id=1, replica_groups=mesh['sp_f'=4,'sp_n'=4,'sp_x'=4,'sp_c'=2,'tp'=4] {'sp_f'}, dimensions={0} | all-to-all | bytes 393216 | tf_op jit(solution)/shard_map/all_to_all | solution.py:49
  32.6 0.7 broadcast_in_dim.20
  33.4 4.6 %all-to-all-start.1 = ((bf16[4,4,16,512]{3,2,1,0:T(8,128)(2,1)}), bf16[4,4,16,512]{3,2,1,0:T(8,128)(2,1)S(1)}, u32[]{:S(2)}, u32[]{:S(2)}) async-start(bf16[4,4,16,512]{3,2,1,0:T(8,128)(2,1)} %broadcast_in_dim.20), calls=%async_computation.1 | async-start | bytes 524288 | tf_op jit(solution)/shard_map/all_to_all | solution.py:49
  38.0 4.2 %collective-permute-start.6 = (bf16[4,16,1024]{2,1,0:T(8,128)(2,1)S(1)}, bf16[4,16,1024]{2,1,0:T(8,128)(2,1)S(1)}, u32[]{:S(2)}, u32[]{:S(2)}) collective-permute-start(bf16[4,16,1024]{2,1,0:T(8,128)(2,1)S(1)} %get-tuple-element.34), channel_id=1, source_target_pairs={{0,448},{32,480},{64,0},{96,32},{128,64},{160,96},{192,128},{224,1... | collective-permute-start | bytes 393224 | tf_op jit(solution)/shard_map/ppermute | solution.py:56
  42.2 2.5 %collective-permute-start.5 = (bf16[4,16,1024]{2,1,0:T(8,128)(2,1)S(1)}, bf16[4,16,1024]{2,1,0:T(8,128)(2,1)S(1)}, u32[]{:S(2)}, u32[]{:S(2)}) collective-permute-start(bf16[4,16,1024]{2,1,0:T(8,128)(2,1)S(1)} %get-tuple-element.34), channel_id=1, source_target_pairs={{0,480},{32,0},{64,32},{96,64},{128,96},{160,128},{192,160},{224,1... | collective-permute-start | bytes 393224 | tf_op jit(solution)/shard_map/ppermute | solution.py:56
  44.6 3.4 %collective-permute-start.4 = (bf16[4,16,1024]{2,1,0:T(8,128)(2,1)S(1)}, bf16[4,16,1024]{2,1,0:T(8,128)(2,1)S(1)}, u32[]{:S(2)}, u32[]{:S(2)}) collective-permute-start(bf16[4,16,1024]{2,1,0:T(8,128)(2,1)S(1)} %get-tuple-element.34), channel_id=1, source_target_pairs={{0,32},{32,64},{64,96},{96,128},{128,160},{160,192},{192,224},{224... | collective-permute-start | bytes 393224 | tf_op jit(solution)/shard_map/ppermute | solution.py:56
  48.0 4.2 %collective-permute-done.6 = bf16[4,16,1024]{2,1,0:T(8,128)(2,1)S(1)} collective-permute-done((bf16[4,16,1024]{2,1,0:T(8,128)(2,1)S(1)}, bf16[4,16,1024]{2,1,0:T(8,128)(2,1)S(1)}, u32[]{:S(2)}, u32[]{:S(2)}) %collective-permute-start.6) | collective-permute-done | bytes 131104 | tf_op jit(solution)/shard_map/ppermute | solution.py:56
  52.2 0.0 collective-permute-done.5
  52.2 0.5 collective-permute-done.4
  52.7 0.9 fusion
  53.6 3.3 %collective-permute-start.9 = (bf16[4,4,16,1024]{3,2,1,0:T(8,128)(2,1)S(1)}, bf16[4,4,16,1024]{3,2,1,0:T(8,128)(2,1)S(1)}, u32[]{:S(2)}, u32[]{:S(2)}) collective-permute-start(bf16[4,4,16,1024]{3,2,1,0:T(8,128)(2,1)S(1)} %get-tuple-element.32), channel_id=1, source_target_pairs={{0,16},{8,24},{16,0},{24,8},{1,17},{9,25},{17,1},{25,9},{2,18},{10... | collective-permute-start | bytes 1572872 | tf_op jit(solution)/shard_map/ppermute | solution.py:56
  56.9 1.9 collective-permute-start.8
  58.8 5.1 %collective-permute-start.7 = (bf16[4,4,16,1024]{3,2,1,0:T(8,128)(2,1)S(1)}, bf16[4,4,16,1024]{3,2,1,0:T(8,128)(2,1)}, u32[]{:S(2)}, u32[]{:S(2)}) collective-permute-start(bf16[4,4,16,1024]{3,2,1,0:T(8,128)(2,1)S(1)} %get-tuple-element.32), channel_id=1, source_target_pairs={{0,8},{8,16},{16,24},{24,0},{1,9},{9,17},{17,25},{25,1},{2,10},{10... | collective-permute-start | bytes 1572872 | tf_op jit(solution)/shard_map/ppermute | solution.py:56
  64.0 0.0 all-to-all-done.1
  64.0 1.1 broadcast_in_dim.21
  65.1 4.5 %all-to-all-start.2 = ((bf16[4,4,4,16,512]{4,3,2,1,0:T(8,128)(2,1)}), bf16[4,4,4,16,512]{4,3,2,1,0:T(8,128)(2,1)S(1)}, u32[]{:S(2)}, u32[]{:S(2)}) async-start(bf16[4,4,4,16,512]{4,3,2,1,0:T(8,128)(2,1)} %broadcast_in_dim.21), calls=%async_computation.2 | async-start | bytes 2097152 | tf_op jit(solution)/shard_map/all_to_all | solution.py:49
  69.6 2.2 collective-permute-done.9
  71.8 0.0 copy-start.2
  71.8 8.7 %collective-permute-done.8 = bf16[4,4,16,1024]{3,2,1,0:T(8,128)(2,1)S(1)} collective-permute-done((bf16[4,4,16,1024]{3,2,1,0:T(8,128)(2,1)S(1)}, bf16[4,4,16,1024]{3,2,1,0:T(8,128)(2,1)S(1)}, u32[]{:S(2)}, u32[]{:S(2)}) %collective-permute-start.8) | collective-permute-done | bytes 524320 | tf_op jit(solution)/shard_map/ppermute | solution.py:56
  80.5 0.0 copy-start.3
  80.5 0.4 collective-permute-done.7
  80.9 0.0 copy-done.2
  80.9 0.4 copy-done.3
  81.3 1.8 pad_maximum_fusion.mine_ref
  83.1 0.0 copy-start
  83.1 1.9 collective-permute-start.10
  85.0 5.5 %all-to-all-done.2.mine_ref = bf16[4,4,4,16,512]{4,3,2,1,0:T(8,128)(2,1)S(1)} async-done(((bf16[4,4,4,16,512]{4,3,2,1,0:T(8,128)(2,1)}), bf16[4,4,4,16,512]{4,3,2,1,0:T(8,128)(2,1)S(1)}, u32[]{:S(2)}, u32[]{:S(2)}) %all-to-all-start.2) | async-done | bytes 1048608 | tf_op jit(solution)/shard_map/all_to_all | solution.py:49
  90.5 0.0 copy-start.1
  90.5 1.9 collective-permute-start.3
  92.5 3.5 %collective-permute-start = (bf16[128,2048]{1,0:T(8,128)(2,1)}, bf16[128,2048]{1,0:T(8,128)(2,1)}, u32[]{:S(2)}, u32[]{:S(2)}) collective-permute-start(bf16[128,2048]{1,0:T(8,128)(2,1)} %own_ref.1), channel_id=1, source_target_pairs={{0,1},{1,2},{2,3},{3,0},{4,5},{5,6},{6,7},{7,4},{8,9},{9,10},{10,1... | collective-permute-start | bytes 1572872 | tf_op jit(solution)/shard_map/ppermute | solution.py:56
  96.0 3.6 %collective-permute-start.1 = (bf16[128,2048]{1,0:T(8,128)(2,1)}, bf16[128,2048]{1,0:T(8,128)(2,1)}, u32[]{:S(2)}, u32[]{:S(2)}) collective-permute-start(bf16[128,2048]{1,0:T(8,128)(2,1)} %own_ref.1), channel_id=1, source_target_pairs={{0,3},{1,0},{2,1},{3,2},{4,7},{5,4},{6,5},{7,6},{8,11},{9,8},{10,9... | collective-permute-start | bytes 1572872 | tf_op jit(solution)/shard_map/ppermute | solution.py:56
  99.5 3.9 %collective-permute-start.2 = (bf16[128,2048]{1,0:T(8,128)(2,1)}, bf16[128,2048]{1,0:T(8,128)(2,1)}, u32[]{:S(2)}, u32[]{:S(2)}) collective-permute-start(bf16[128,2048]{1,0:T(8,128)(2,1)} %own_ref.1), channel_id=1, source_target_pairs={{0,2},{1,3},{2,0},{3,1},{4,6},{5,7},{6,4},{7,5},{8,10},{9,11},{10,... | collective-permute-start | bytes 1572872 | tf_op jit(solution)/shard_map/ppermute | solution.py:56
  103.5 0.6 stack.57.info_ref
  104.1 6.2 %collective-permute-done.before_ref = bf16[128,2048]{1,0:T(8,128)(2,1)} collective-permute-done((bf16[128,2048]{1,0:T(8,128)(2,1)}, bf16[128,2048]{1,0:T(8,128)(2,1)}, u32[]{:S(2)}, u32[]{:S(2)}) %collective-permute-start) | collective-permute-done | bytes 524320 | tf_op jit(solution)/shard_map/ppermute | solution.py:56
  110.3 2.7 %collective-permute-done.1.after_ref = bf16[128,2048]{1,0:T(8,128)(2,1)} collective-permute-done((bf16[128,2048]{1,0:T(8,128)(2,1)}, bf16[128,2048]{1,0:T(8,128)(2,1)}, u32[]{:S(2)}, u32[]{:S(2)}) %collective-permute-start.1) | collective-permute-done | bytes 524320 | tf_op jit(solution)/shard_map/ppermute | solution.py:56
  113.0 9.7 %collective-permute-done.2.far_ref = bf16[128,2048]{1,0:T(8,128)(2,1)} collective-permute-done((bf16[128,2048]{1,0:T(8,128)(2,1)}, bf16[128,2048]{1,0:T(8,128)(2,1)}, u32[]{:S(2)}, u32[]{:S(2)}) %collective-permute-start.2) | collective-permute-done | bytes 524320 | tf_op jit(solution)/shard_map/ppermute | solution.py:56
  122.7 0.0 collective-permute-done.3.other_ref
  122.7 0.0 copy-done.1
  122.7 7.7 %shard_map.109 = (bf16[512,2048]{1,0:T(8,128)(2,1)}, bf16[512,256]{1,0:T(8,128)(2,1)}, f32[512,256]{1,0:T(8,128)}, f32[512,256]{1,0:T(8,128)}, f32[4,128,256]{2,1,0:T(8,128)}, /*index=5*/bf16[8,24,256]{2,1,0:T(8,128)(2,1)}) custom-call(s32[6]{0:T(128)} %stack.57.info_ref, bf16[128,2048]{1,0:T(8,128)(2,1)} %own_ref.1, ...), custom_call_target="tpu_custom_call" | custom-call | flops 1073741824 | bytes 8388608 | tf_op jit(solution)/shard_map/pallas_call | solution.py:372
  130.4 0.0 copy-done
  130.4 8.6 %all_to_all.39.got_ref = bf16[8,24,256]{2,1,0:T(8,128)(2,1)} all-to-all(bf16[8,24,256]{2,1,0:T(8,128)(2,1)} %get-tuple-element.18), channel_id=1, replica_groups=mesh['sp_f'=4,'sp_n'=4,'sp_x'=4,'sp_c'=2,'tp'=4] {'sp_x','sp_c'}, dimensions={0} | all-to-all | bytes 196608 | tf_op jit(solution)/shard_map/all_to_all | solution.py:481
  139.1 1.7 shard_map.110
  140.7 22.8 %all_to_all.40.totals_ref = bf16[16,24,256]{2,1,0:T(8,128)(2,1)} all-to-all(bf16[16,24,256]{2,1,0:T(8,128)(2,1)} %get-tuple-element.19), channel_id=1, replica_groups=mesh['sp_f'=4,'sp_n'=4,'sp_x'=4,'sp_c'=2,'tp'=4] {'sp_f','sp_n'}, dimensions={0} | all-to-all | bytes 393216 | tf_op jit(solution)/shard_map/all_to_all | solution.py:494
  163.5 1.7 shard_map.111
  165.2 5.4 %all-to-all-start.5 = ((bf16[8,16,256]{2,1,0:T(8,128)(2,1)}), bf16[8,16,256]{2,1,0:T(8,128)(2,1)S(1)}, u32[]{:S(2)}, u32[]{:S(2)}) async-start(bf16[8,16,256]{2,1,0:T(8,128)(2,1)} %shard_map.111), calls=%async_computation.5 | async-start | bytes 131072 | tf_op jit(solution)/shard_map/all_to_all | solution.py:506
  170.6 0.0 collective-permute-done.10.other_ref
  170.6 7.7 %shard_map.112 = (bf16[512,256]{1,0:T(8,128)(2,1)}, bf16[16,256]{1,0:T(8,128)(2,1)}, f32[512,256]{1,0:T(8,128)}, f32[512,256]{1,0:T(8,128)}) custom-call(s32[6]{0:T(128)} %stack.57.info_ref, bf16[512,2048]{1,0:T(8,128)(2,1)} %get-tuple-element.24.normed_ref, bf16[4,4,4,16,1024]{4,3,2,1,0:T(8,128)(2,1)} %copy-done, ...), custom_call_target="tpu_custom_call" | custom-call | flops 1073741824 | bytes 8388608 | tf_op jit(solution)/shard_map/pallas_call | solution.py:372
  178.3 2.0 collective-permute-start.11
  180.3 3.1 %collective-permute-done.11.rim_ref = bf16[16,256]{1,0:T(8,128)(2,1)S(1)} collective-permute-done((bf16[16,256]{1,0:T(8,128)(2,1)}, bf16[16,256]{1,0:T(8,128)(2,1)S(1)}, u32[]{:S(2)}, u32[]{:S(2)}) %collective-permute-start.11) | collective-permute-done | bytes 8224 | tf_op jit(solution)/shard_map/ppermute | solution.py:534
  183.5 0.0 copy-start.5
  183.5 0.6 copy-done.5
  184.1 2.0 shard_map.113.pool_ref
  186.1 0.0 all-to-all-done.5
  186.1 0.0 copy-start.4
  186.1 0.6 copy-done.4
  186.7 5.7 %shard_map.114 = bf16[512,2048]{1,0:T(8,128)(2,1)} custom-call(s32[6]{0:T(128)} %stack.57.info_ref, bf16[128,256]{1,0:T(8,128)(2,1)} %bitcast.26, f32[4,128,256]{2,1,0:T(8,128)} %get-tuple-element.22.growth_ref, f32[512,256]{1,0:T(8,128)} %get-tuple-element.23.cum_ref, f32[512,256]{1,0:T(8,128)} %get-tuple-element.27.decayed_ref, ...), custom_call_target="tpu_custom_call" | custom-call | flops 1073741824 | bytes 8388608 | tf_op jit(solution)/shard_map/pallas_call | solution.py:372
  192.4 29.9 %all_to_all.41 = bf16[4,128,2048]{2,1,0:T(8,128)(2,1)S(1)} all-to-all(bf16[4,128,2048]{2,1,0:T(8,128)(2,1)} %bitcast.23), channel_id=1, replica_groups=mesh['sp_f'=4,'sp_n'=4,'sp_x'=4,'sp_c'=2,'tp'=4] {'tp'}, dimensions={0} | all-to-all | bytes 4194304 | tf_op jit(solution)/shard_map/all_to_all | solution.py:559
  222.3 1.3 reduce_sum.12
  (3 shorter events, 0.0 us)
Async XLA Ops:
  33.4 30.6 %all-to-all-start.1 = ((bf16[4,4,16,512]{3,2,1,0:T(8,128)(2,1)}), bf16[4,4,16,512]{3,2,1,0:T(8,128)(2,1)S(1)}, u32[]{:S(2)}, u32[]{:S(2)}) async-start(bf16[4,4,16,512]{3,2,1,0:T(8,128)(2,1)} %broadcast_in_dim.20), calls=%async_computation.1 | async-start | bytes 524288 | tf_op jit(solution)/shard_map/all_to_all | solution.py:49
  38.0 14.2 %collective-permute-start.6 = (bf16[4,16,1024]{2,1,0:T(8,128)(2,1)S(1)}, bf16[4,16,1024]{2,1,0:T(8,128)(2,1)S(1)}, u32[]{:S(2)}, u32[]{:S(2)}) collective-permute-start(bf16[4,16,1024]{2,1,0:T(8,128)(2,1)S(1)} %get-tuple-element.34), channel_id=1, source_target_pairs={{0,448},{32,480},{64,0},{96,32},{128,64},{160,96},{192,128},{224,1... | collective-permute-start | bytes 393224 | tf_op jit(solution)/shard_map/ppermute | solution.py:56
  42.2 10.1 %collective-permute-start.5 = (bf16[4,16,1024]{2,1,0:T(8,128)(2,1)S(1)}, bf16[4,16,1024]{2,1,0:T(8,128)(2,1)S(1)}, u32[]{:S(2)}, u32[]{:S(2)}) collective-permute-start(bf16[4,16,1024]{2,1,0:T(8,128)(2,1)S(1)} %get-tuple-element.34), channel_id=1, source_target_pairs={{0,480},{32,0},{64,32},{96,64},{128,96},{160,128},{192,160},{224,1... | collective-permute-start | bytes 393224 | tf_op jit(solution)/shard_map/ppermute | solution.py:56
  44.6 8.1 %collective-permute-start.4 = (bf16[4,16,1024]{2,1,0:T(8,128)(2,1)S(1)}, bf16[4,16,1024]{2,1,0:T(8,128)(2,1)S(1)}, u32[]{:S(2)}, u32[]{:S(2)}) collective-permute-start(bf16[4,16,1024]{2,1,0:T(8,128)(2,1)S(1)} %get-tuple-element.34), channel_id=1, source_target_pairs={{0,32},{32,64},{64,96},{96,128},{128,160},{160,192},{192,224},{224... | collective-permute-start | bytes 393224 | tf_op jit(solution)/shard_map/ppermute | solution.py:56
  53.6 18.2 %collective-permute-start.9 = (bf16[4,4,16,1024]{3,2,1,0:T(8,128)(2,1)S(1)}, bf16[4,4,16,1024]{3,2,1,0:T(8,128)(2,1)S(1)}, u32[]{:S(2)}, u32[]{:S(2)}) collective-permute-start(bf16[4,4,16,1024]{3,2,1,0:T(8,128)(2,1)S(1)} %get-tuple-element.32), channel_id=1, source_target_pairs={{0,16},{8,24},{16,0},{24,8},{1,17},{9,25},{17,1},{25,9},{2,18},{10... | collective-permute-start | bytes 1572872 | tf_op jit(solution)/shard_map/ppermute | solution.py:56
  56.9 23.6 %collective-permute-start.8 = (bf16[4,4,16,1024]{3,2,1,0:T(8,128)(2,1)S(1)}, bf16[4,4,16,1024]{3,2,1,0:T(8,128)(2,1)S(1)}, u32[]{:S(2)}, u32[]{:S(2)}) collective-permute-start(bf16[4,4,16,1024]{3,2,1,0:T(8,128)(2,1)S(1)} %get-tuple-element.32), channel_id=1, source_target_pairs={{0,24},{8,0},{16,8},{24,16},{1,25},{9,1},{17,9},{25,17},{2,26},{10... | collective-permute-start | bytes 1572872 | tf_op jit(solution)/shard_map/ppermute | solution.py:56
  58.8 22.1 %collective-permute-start.7 = (bf16[4,4,16,1024]{3,2,1,0:T(8,128)(2,1)S(1)}, bf16[4,4,16,1024]{3,2,1,0:T(8,128)(2,1)}, u32[]{:S(2)}, u32[]{:S(2)}) collective-permute-start(bf16[4,4,16,1024]{3,2,1,0:T(8,128)(2,1)S(1)} %get-tuple-element.32), channel_id=1, source_target_pairs={{0,8},{8,16},{16,24},{24,0},{1,9},{9,17},{17,25},{25,1},{2,10},{10... | collective-permute-start | bytes 1572872 | tf_op jit(solution)/shard_map/ppermute | solution.py:56
  65.1 25.4 %all-to-all-start.2 = ((bf16[4,4,4,16,512]{4,3,2,1,0:T(8,128)(2,1)}), bf16[4,4,4,16,512]{4,3,2,1,0:T(8,128)(2,1)S(1)}, u32[]{:S(2)}, u32[]{:S(2)}) async-start(bf16[4,4,4,16,512]{4,3,2,1,0:T(8,128)(2,1)} %broadcast_in_dim.21), calls=%async_computation.2 | async-start | bytes 2097152 | tf_op jit(solution)/shard_map/all_to_all | solution.py:49
  71.8 9.1 %copy-start.2 = (bf16[4,4,16,1024]{3,2,1,0:T(8,128)(2,1)}, bf16[4,4,16,1024]{3,2,1,0:T(8,128)(2,1)S(1)}, u32[]{:S(2)}) copy-start(bf16[4,4,16,1024]{3,2,1,0:T(8,128)(2,1)S(1)} %collective-permute-done.9) | copy-start | bytes 1572868
  80.5 0.8 copy-start.3
  83.1 47.3 %copy-start = (bf16[4,4,4,16,1024]{4,3,2,1,0:T(8,128)(2,1)}, bf16[4,4,4,16,1024]{4,3,2,1,0:T(8,128)(2,1)S(1)}, u32[]{:S(2)}) copy-start(bf16[4,4,4,16,1024]{4,3,2,1,0:T(8,128)(2,1)S(1)} %pad_maximum_fusion.mine_ref) | copy-start | bytes 6291460
  83.1 87.5 %collective-permute-start.10 = (bf16[4,4,4,16,1024]{4,3,2,1,0:T(8,128)(2,1)S(1)}, bf16[4,4,4,16,1024]{4,3,2,1,0:T(8,128)(2,1)}, u32[]{:S(2)}, u32[]{:S(2)}) collective-permute-start(bf16[4,4,4,16,1024]{4,3,2,1,0:T(8,128)(2,1)S(1)} %pad_maximum_fusion.mine_ref), channel_id=1, source_target_pairs={{0,4},{4,0},{1,5},{5,1},{2,6},{6,2},{3,7},{7,3},{8,12},{12,8},{9,1... | collective-permute-start | bytes 6291464 | tf_op jit(solution)/shard_map/ppermute | solution.py:397
  90.5 32.2 %copy-start.1 = (bf16[4,4,4,16,512]{4,3,2,1,0:T(8,128)(2,1)}, bf16[4,4,4,16,512]{4,3,2,1,0:T(8,128)(2,1)S(1)}, u32[]{:S(2)}) copy-start(bf16[4,4,4,16,512]{4,3,2,1,0:T(8,128)(2,1)S(1)} %all-to-all-done.2.mine_ref) | copy-start | bytes 3145732
  90.5 32.1 %collective-permute-start.3 = (bf16[4,4,4,16,512]{4,3,2,1,0:T(8,128)(2,1)S(1)}, bf16[4,4,4,16,512]{4,3,2,1,0:T(8,128)(2,1)}, u32[]{:S(2)}, u32[]{:S(2)}) collective-permute-start(bf16[4,4,4,16,512]{4,3,2,1,0:T(8,128)(2,1)S(1)} %all-to-all-done.2.mine_ref), channel_id=1, source_target_pairs={{0,4},{4,0},{1,5},{5,1},{2,6},{6,2},{3,7},{7,3},{8,12},{12,8},{9,1... | collective-permute-start | bytes 3145736 | tf_op jit(solution)/shard_map/ppermute | solution.py:397
  92.5 17.8 %collective-permute-start = (bf16[128,2048]{1,0:T(8,128)(2,1)}, bf16[128,2048]{1,0:T(8,128)(2,1)}, u32[]{:S(2)}, u32[]{:S(2)}) collective-permute-start(bf16[128,2048]{1,0:T(8,128)(2,1)} %own_ref.1), channel_id=1, source_target_pairs={{0,1},{1,2},{2,3},{3,0},{4,5},{5,6},{6,7},{7,4},{8,9},{9,10},{10,1... | collective-permute-start | bytes 1572872 | tf_op jit(solution)/shard_map/ppermute | solution.py:56
  96.0 17.0 %collective-permute-start.1 = (bf16[128,2048]{1,0:T(8,128)(2,1)}, bf16[128,2048]{1,0:T(8,128)(2,1)}, u32[]{:S(2)}, u32[]{:S(2)}) collective-permute-start(bf16[128,2048]{1,0:T(8,128)(2,1)} %own_ref.1), channel_id=1, source_target_pairs={{0,3},{1,0},{2,1},{3,2},{4,7},{5,4},{6,5},{7,6},{8,11},{9,8},{10,9... | collective-permute-start | bytes 1572872 | tf_op jit(solution)/shard_map/ppermute | solution.py:56
  99.5 23.2 %collective-permute-start.2 = (bf16[128,2048]{1,0:T(8,128)(2,1)}, bf16[128,2048]{1,0:T(8,128)(2,1)}, u32[]{:S(2)}, u32[]{:S(2)}) collective-permute-start(bf16[128,2048]{1,0:T(8,128)(2,1)} %own_ref.1), channel_id=1, source_target_pairs={{0,2},{1,3},{2,0},{3,1},{4,6},{5,7},{6,4},{7,5},{8,10},{9,11},{10,... | collective-permute-start | bytes 1572872 | tf_op jit(solution)/shard_map/ppermute | solution.py:56
  165.2 20.8 %all-to-all-start.5 = ((bf16[8,16,256]{2,1,0:T(8,128)(2,1)}), bf16[8,16,256]{2,1,0:T(8,128)(2,1)S(1)}, u32[]{:S(2)}, u32[]{:S(2)}) async-start(bf16[8,16,256]{2,1,0:T(8,128)(2,1)} %shard_map.111), calls=%async_computation.5 | async-start | bytes 131072 | tf_op jit(solution)/shard_map/all_to_all | solution.py:506
  178.3 5.2 %collective-permute-start.11 = (bf16[16,256]{1,0:T(8,128)(2,1)}, bf16[16,256]{1,0:T(8,128)(2,1)S(1)}, u32[]{:S(2)}, u32[]{:S(2)}) collective-permute-start(bf16[16,256]{1,0:T(8,128)(2,1)} %get-tuple-element.30), channel_id=1, source_target_pairs={{0,4},{4,8},{8,12},{12,16},{16,20},{20,24},{24,28},{28,32},{32,36}... | collective-permute-start | bytes 24584 | tf_op jit(solution)/shard_map/ppermute | solution.py:534
  183.5 0.6 copy-start.5
  186.1 0.6 copy-start.4

commit v2 on v1

--- a/solution.py
+++ b/solution.py
@@ -115,6 +115,7 @@
     cum_ref,
     growth_ref,
     payload_ref,
+    edge_ref,
     whole_ref,
     sems,
     both_ref,
@@ -152,6 +153,7 @@
             normed_ref[at, :] = (floats * scale * gain_ref[...]).astype(BF)
     handing = pltpu.make_async_copy(normed_ref, normed_out_ref, token_sems.at[len(spots)])
     handing.start()
+    edge_ref[...] = normed_ref[rows - RIM :, :]
     finished(copies)
     both_ref[...] = dot(normed_ref[...], whole_ref[...].reshape(-1, 2 * cols))
     row = lax.broadcasted_iota(jnp.int32, (CHUNK, CHUNK), 0)
@@ -239,6 +241,7 @@
     values_ref,
     opened_ref,
     cum_ref,
+    rim_ref,
     pooled_ref,
     edge_ref,
     decayed_ref,
@@ -267,7 +270,7 @@
     bringing.wait()
     both_ref[...] = dot(held_ref[...], whole_ref[...].reshape(-1, 2 * cols))
     pooled_ref[...] = both_ref[:, cols:].astype(BF)
-    edge_ref[...] = both_ref[rows - RIM :, cols:].astype(BF)
+    edge_ref[...] = dot(rim_ref[...], whole_ref[..., cols:].reshape(-1, cols)).astype(BF)
     row = lax.broadcasted_iota(jnp.int32, (CHUNK, CHUNK), 0)
     col = lax.broadcasted_iota(jnp.int32, (CHUNK, CHUNK), 1)
     for h in range(cols // RDIM):
@@ -450,7 +453,7 @@
 
     plane = lax.axis_size(PLANE)
     slab = RDIM // plane
-    normed, values, opened, cum, growth, payload = call(
+    normed, values, opened, cum, growth, payload, edge = call(
         state_kernel,
         [
             shape((rows, width), BF),
@@ -459,6 +462,7 @@
             shape((rows, cols), F32),
             shape((rows // CHUNK, RDIM, cols), F32),
             shape((plane, slab + 8, cols), BF),
+            shape((RIM, width), BF),
         ],
         [
             *whole,
@@ -476,8 +480,10 @@
         first_other,
         forget_gap[None, :],
         decay_shift,
-        out_specs=[HBM, VMEM, VMEM, VMEM, VMEM, VMEM],
-    )
+        out_specs=[HBM, VMEM, VMEM, VMEM, VMEM, VMEM, VMEM],
+    )
+    order = [(i - 1, i) for i in range(1, devices)]
+    rim = lax.ppermute(edge, SP, order)
     got = lax.all_to_all(payload, PLANE, split_axis=0, concat_axis=0, tiled=True)
     before, faded, total = call(
         plane_kernel,
@@ -506,7 +512,7 @@
     start = lax.all_to_all(
         start.reshape(RDIM, cols), PLANE, split_axis=0, concat_axis=0, tiled=True
     )
-    pooled, edge, decayed, heard = call(
+    pooled, before_pooled, decayed, heard = call(
         inner_kernel,
         [
             shape((rows, cols), BF),
@@ -529,10 +535,11 @@
         values,
         opened,
         cum,
-    )
-    order = [(i - 1, i) for i in range(1, devices)]
-    rim = lax.ppermute(edge, SP, order)
-    pool = call(pool_kernel, shape((rows, cols), BF), [], 1 << 20, 1 << 19, info, pooled, rim)
+        rim,
+    )
+    pool = call(
+        pool_kernel, shape((rows, cols), BF), [], 1 << 20, 1 << 19, info, pooled, before_pooled
+    )
     part = call(
         final_kernel,
         shape((rows, width), BF),

time: 226 us -> 222 us (0.982)
  blocking collectives: 93.1 us -> 72.1 us
  waiting for transfers between devices: 43.3 us -> 54.6 us
  starting transfers between devices: 51.6 us -> 57.8 us
    all_to_all x1 -> x0, blocking collectives: 22.8 us -> none  [layer(): lax.all_to_all(total, DEPTH, split_axis=0, concat_axis=0, tiled=True)]
    all_to_all x0 -> x1, waiting for transfers between devices: none -> 14.5 us  [layer(): lax.all_to_all(total, DEPTH, split_axis=0, concat_axis=0, tiled=True)]
    all_to_all x0 -> x1, starting transfers between devices: none -> 6.48 us  [layer(): lax.all_to_all(total, DEPTH, split_axis=0, concat_axis=0, tiled=True)]
    ppermute x1, waiting for transfers between devices: 3.14 us -> 0.01 us  [layer(): rim = lax.ppermute(edge, SP, order)]
  transfers between devices with their start and end apart: 15 -> 16, of which waited for: 10 -> 10; matrix products, arithmetic and copies ran while one was open for 2% -> 2% of each run, Pallas kernels for 9% -> 9%
where the time goes in v2:
time: 222 us; the launch traced here: 221 us
  blocking collectives  72.1 us (32%)
  starting transfers between devices  57.8 us (26%)
  waiting for transfers between devices  54.6 us (25%)
  Pallas kernels  26.3 us (12%)
  local copies, waits for them, and re-layouts  4.83 us (2%)
  other arithmetic  4.75 us (2%)
    ppermute x9, waiting for transfers between devices, ring_gather(): lax.ppermute(x, axis, [(i, (i + shift) % n) for i in range(n)])  34.5 us
    all_to_all x1, blocking collectives, sent_to_all(): return lax.all_to_all(copies, axis, split_axis=0, concat_axis=0, tiled=True)  31.8 us
    all_to_all x1, blocking collectives, layer(): lax.all_to_all(part.reshape(tp, rows // tp, width), 'tp', split_axis=0, c...  31.6 us
    ppermute x9, starting transfers between devices, ring_gather(): lax.ppermute(x, axis, [(i, (i + shift) % n) for i in range(n)])  31.3 us
    pallas_call x6, Pallas kernels, call(): pl.pallas_call(kernel, out_shape=outs, in_specs=[spec_of(a) for a in args...  26.3 us
    all_to_all x1, waiting for transfers between devices, layer(): lax.all_to_all(total, DEPTH, split_axis=0, concat_axis=0, tiled=True)  14.5 us
    all_to_all x2, starting transfers between devices, sent_to_all(): return lax.all_to_all(copies, axis, split_axis=0, concat_axis=0, tiled=True)  9.12 us
    all_to_all x1, blocking collectives, layer(): lax.all_to_all(payload, PLANE, split_axis=0, concat_axis=0, tiled=True)  8.62 us
  transfers between devices with their start and end apart: 16, of which 10 were waited for; matrix products, arithmetic and copies ran while one was open for 2% of the time, Pallas kernels for 9%

profile of v2, /device:TPU:6, one launch (start us, length us, event | category | flops | bytes accessed | tf_op | source)
XLA Modules:
  0.0 220.6 jit_solution(9592219367453352519)
XLA Ops:
  0.0 0.8 pad_add_fusion
  0.8 31.8 %all_to_all.38 = bf16[4,16,1536]{2,1,0:T(8,128)(2,1)S(1)} all-to-all(bf16[4,16,1536]{2,1,0:T(8,128)(2,1)S(1)} %broadcast_in_dim.19), channel_id=1, replica_groups=mesh['sp_f'=4,'sp_n'=4,'sp_x'=4,'sp_c'=2,'tp'=4] {'sp_f'}, dimensions={0} | all-to-all | bytes 393216 | tf_op jit(solution)/shard_map/all_to_all | solution.py:49
  32.6 0.7 broadcast_in_dim.20
  33.4 4.6 %all-to-all-start.1 = ((bf16[4,4,16,512]{3,2,1,0:T(8,128)(2,1)}), bf16[4,4,16,512]{3,2,1,0:T(8,128)(2,1)S(1)}, u32[]{:S(2)}, u32[]{:S(2)}) async-start(bf16[4,4,16,512]{3,2,1,0:T(8,128)(2,1)} %broadcast_in_dim.20), calls=%async_computation.1 | async-start | bytes 524288 | tf_op jit(solution)/shard_map/all_to_all | solution.py:49
  38.0 4.2 %collective-permute-start.6 = (bf16[4,16,1024]{2,1,0:T(8,128)(2,1)S(1)}, bf16[4,16,1024]{2,1,0:T(8,128)(2,1)S(1)}, u32[]{:S(2)}, u32[]{:S(2)}) collective-permute-start(bf16[4,16,1024]{2,1,0:T(8,128)(2,1)S(1)} %get-tuple-element.36), channel_id=1, source_target_pairs={{0,448},{32,480},{64,0},{96,32},{128,64},{160,96},{192,128},{224,1... | collective-permute-start | bytes 393224 | tf_op jit(solution)/shard_map/ppermute | solution.py:56
  42.2 2.5 %collective-permute-start.5 = (bf16[4,16,1024]{2,1,0:T(8,128)(2,1)S(1)}, bf16[4,16,1024]{2,1,0:T(8,128)(2,1)S(1)}, u32[]{:S(2)}, u32[]{:S(2)}) collective-permute-start(bf16[4,16,1024]{2,1,0:T(8,128)(2,1)S(1)} %get-tuple-element.36), channel_id=1, source_target_pairs={{0,480},{32,0},{64,32},{96,64},{128,96},{160,128},{192,160},{224,1... | collective-permute-start | bytes 393224 | tf_op jit(solution)/shard_map/ppermute | solution.py:56
  44.7 3.4 %collective-permute-start.4 = (bf16[4,16,1024]{2,1,0:T(8,128)(2,1)S(1)}, bf16[4,16,1024]{2,1,0:T(8,128)(2,1)S(1)}, u32[]{:S(2)}, u32[]{:S(2)}) collective-permute-start(bf16[4,16,1024]{2,1,0:T(8,128)(2,1)S(1)} %get-tuple-element.36), channel_id=1, source_target_pairs={{0,32},{32,64},{64,96},{96,128},{128,160},{160,192},{192,224},{224... | collective-permute-start | bytes 393224 | tf_op jit(solution)/shard_map/ppermute | solution.py:56
  48.0 4.2 %collective-permute-done.6 = bf16[4,16,1024]{2,1,0:T(8,128)(2,1)S(1)} collective-permute-done((bf16[4,16,1024]{2,1,0:T(8,128)(2,1)S(1)}, bf16[4,16,1024]{2,1,0:T(8,128)(2,1)S(1)}, u32[]{:S(2)}, u32[]{:S(2)}) %collective-permute-start.6) | collective-permute-done | bytes 131104 | tf_op jit(solution)/shard_map/ppermute | solution.py:56
  52.3 0.0 collective-permute-done.5
  52.3 0.5 collective-permute-done.4
  52.7 0.9 fusion
  53.6 3.3 %collective-permute-start.9 = (bf16[4,4,16,1024]{3,2,1,0:T(8,128)(2,1)S(1)}, bf16[4,4,16,1024]{3,2,1,0:T(8,128)(2,1)S(1)}, u32[]{:S(2)}, u32[]{:S(2)}) collective-permute-start(bf16[4,4,16,1024]{3,2,1,0:T(8,128)(2,1)S(1)} %get-tuple-element.34), channel_id=1, source_target_pairs={{0,16},{8,24},{16,0},{24,8},{1,17},{9,25},{17,1},{25,9},{2,18},{10... | collective-permute-start | bytes 1572872 | tf_op jit(solution)/shard_map/ppermute | solution.py:56
  56.9 1.9 collective-permute-start.8
  58.9 5.1 %collective-permute-start.7 = (bf16[4,4,16,1024]{3,2,1,0:T(8,128)(2,1)S(1)}, bf16[4,4,16,1024]{3,2,1,0:T(8,128)(2,1)}, u32[]{:S(2)}, u32[]{:S(2)}) collective-permute-start(bf16[4,4,16,1024]{3,2,1,0:T(8,128)(2,1)S(1)} %get-tuple-element.34), channel_id=1, source_target_pairs={{0,8},{8,16},{16,24},{24,0},{1,9},{9,17},{17,25},{25,1},{2,10},{10... | collective-permute-start | bytes 1572872 | tf_op jit(solution)/shard_map/ppermute | solution.py:56
  64.0 0.0 all-to-all-done.1
  64.0 1.1 broadcast_in_dim.21
  65.2 4.5 %all-to-all-start.2 = ((bf16[4,4,4,16,512]{4,3,2,1,0:T(8,128)(2,1)}), bf16[4,4,4,16,512]{4,3,2,1,0:T(8,128)(2,1)S(1)}, u32[]{:S(2)}, u32[]{:S(2)}) async-start(bf16[4,4,4,16,512]{4,3,2,1,0:T(8,128)(2,1)} %broadcast_in_dim.21), calls=%async_computation.2 | async-start | bytes 2097152 | tf_op jit(solution)/shard_map/all_to_all | solution.py:49
  69.7 2.2 collective-permute-done.9
  71.8 0.0 copy-start.3
  71.8 8.7 %collective-permute-done.8 = bf16[4,4,16,1024]{3,2,1,0:T(8,128)(2,1)S(1)} collective-permute-done((bf16[4,4,16,1024]{3,2,1,0:T(8,128)(2,1)S(1)}, bf16[4,4,16,1024]{3,2,1,0:T(8,128)(2,1)S(1)}, u32[]{:S(2)}, u32[]{:S(2)}) %collective-permute-start.8) | collective-permute-done | bytes 524320 | tf_op jit(solution)/shard_map/ppermute | solution.py:56
  80.5 0.0 copy-start.4
  80.5 0.4 collective-permute-done.7
  80.9 0.0 copy-done.3
  81.0 0.4 copy-done.4
  81.3 1.8 pad_maximum_fusion.mine_ref
  83.1 0.0 copy-start
  83.1 1.9 collective-permute-start.10
  85.0 5.5 %all-to-all-done.2.mine_ref = bf16[4,4,4,16,512]{4,3,2,1,0:T(8,128)(2,1)S(1)} async-done(((bf16[4,4,4,16,512]{4,3,2,1,0:T(8,128)(2,1)}), bf16[4,4,4,16,512]{4,3,2,1,0:T(8,128)(2,1)S(1)}, u32[]{:S(2)}, u32[]{:S(2)}) %all-to-all-start.2) | async-done | bytes 1048608 | tf_op jit(solution)/shard_map/all_to_all | solution.py:49
  90.6 0.0 copy-start.1
  90.6 1.9 collective-permute-start.3
  92.5 3.5 %collective-permute-start = (bf16[128,2048]{1,0:T(8,128)(2,1)}, bf16[128,2048]{1,0:T(8,128)(2,1)}, u32[]{:S(2)}, u32[]{:S(2)}) collective-permute-start(bf16[128,2048]{1,0:T(8,128)(2,1)} %own_ref.1), channel_id=1, source_target_pairs={{0,1},{1,2},{2,3},{3,0},{4,5},{5,6},{6,7},{7,4},{8,9},{9,10},{10,1... | collective-permute-start | bytes 1572872 | tf_op jit(solution)/shard_map/ppermute | solution.py:56
  96.0 3.6 %collective-permute-start.1 = (bf16[128,2048]{1,0:T(8,128)(2,1)}, bf16[128,2048]{1,0:T(8,128)(2,1)}, u32[]{:S(2)}, u32[]{:S(2)}) collective-permute-start(bf16[128,2048]{1,0:T(8,128)(2,1)} %own_ref.1), channel_id=1, source_target_pairs={{0,3},{1,0},{2,1},{3,2},{4,7},{5,4},{6,5},{7,6},{8,11},{9,8},{10,9... | collective-permute-start | bytes 1572872 | tf_op jit(solution)/shard_map/ppermute | solution.py:56
  99.6 3.9 %collective-permute-start.2 = (bf16[128,2048]{1,0:T(8,128)(2,1)}, bf16[128,2048]{1,0:T(8,128)(2,1)}, u32[]{:S(2)}, u32[]{:S(2)}) collective-permute-start(bf16[128,2048]{1,0:T(8,128)(2,1)} %own_ref.1), channel_id=1, source_target_pairs={{0,2},{1,3},{2,0},{3,1},{4,6},{5,7},{6,4},{7,5},{8,10},{9,11},{10,... | collective-permute-start | bytes 1572872 | tf_op jit(solution)/shard_map/ppermute | solution.py:56
  103.5 0.7 stack.57.info_ref
  104.1 6.2 %collective-permute-done.before_ref = bf16[128,2048]{1,0:T(8,128)(2,1)} collective-permute-done((bf16[128,2048]{1,0:T(8,128)(2,1)}, bf16[128,2048]{1,0:T(8,128)(2,1)}, u32[]{:S(2)}, u32[]{:S(2)}) %collective-permute-start) | collective-permute-done | bytes 524320 | tf_op jit(solution)/shard_map/ppermute | solution.py:56
  110.3 2.7 %collective-permute-done.1.after_ref = bf16[128,2048]{1,0:T(8,128)(2,1)} collective-permute-done((bf16[128,2048]{1,0:T(8,128)(2,1)}, bf16[128,2048]{1,0:T(8,128)(2,1)}, u32[]{:S(2)}, u32[]{:S(2)}) %collective-permute-start.1) | collective-permute-done | bytes 524320 | tf_op jit(solution)/shard_map/ppermute | solution.py:56
  113.0 9.7 %collective-permute-done.2.far_ref = bf16[128,2048]{1,0:T(8,128)(2,1)} collective-permute-done((bf16[128,2048]{1,0:T(8,128)(2,1)}, bf16[128,2048]{1,0:T(8,128)(2,1)}, u32[]{:S(2)}, u32[]{:S(2)}) %collective-permute-start.2) | collective-permute-done | bytes 524320 | tf_op jit(solution)/shard_map/ppermute | solution.py:56
  122.7 0.0 collective-permute-done.3.other_ref
  122.7 0.0 copy-done.1
  122.7 7.7 %shard_map.109 = (bf16[512,2048]{1,0:T(8,128)(2,1)}, bf16[512,256]{1,0:T(8,128)(2,1)}, f32[512,256]{1,0:T(8,128)}, f32[512,256]{1,0:T(8,128)}, f32[4,128,256]{2,...) custom-call(s32[6]{0:T(128)} %stack.57.info_ref, bf16[128,2048]{1,0:T(8,128)(2,1)} %own_ref.1, ...), custom_call_target="tpu_custom_call" | custom-call | flops 1073741824 | bytes 8388608 | tf_op jit(solution)/shard_map/pallas_call | solution.py:375
  130.5 0.0 copy-done
  130.5 8.6 %all_to_all.39.got_ref = bf16[8,24,256]{2,1,0:T(8,128)(2,1)} all-to-all(bf16[8,24,256]{2,1,0:T(8,128)(2,1)} %get-tuple-element.19), channel_id=1, replica_groups=mesh['sp_f'=4,'sp_n'=4,'sp_x'=4,'sp_c'=2,'tp'=4] {'sp_x','sp_c'}, dimensions={0} | all-to-all | bytes 196608 | tf_op jit(solution)/shard_map/all_to_all | solution.py:487
  139.1 1.7 shard_map.110
  140.8 6.5 %all-to-all-start.4 = ((bf16[16,24,256]{2,1,0:T(8,128)(2,1)}), bf16[16,24,256]{2,1,0:T(8,128)(2,1)S(1)}, u32[]{:S(2)}, u32[]{:S(2)}) async-start(bf16[16,24,256]{2,1,0:T(8,128)(2,1)} %get-tuple-element.20), calls=%async_computation.4 | async-start | bytes 393216 | tf_op jit(solution)/shard_map/all_to_all | solution.py:500
  147.2 1.9 collective-permute-start.11
  149.2 14.5 %all-to-all-done.4.totals_ref = bf16[16,24,256]{2,1,0:T(8,128)(2,1)S(1)} async-done(((bf16[16,24,256]{2,1,0:T(8,128)(2,1)}), bf16[16,24,256]{2,1,0:T(8,128)(2,1)S(1)}, u32[]{:S(2)}, u32[]{:S(2)}) %all-to-all-start.4) | async-done | bytes 196640 | tf_op jit(solution)/shard_map/all_to_all | solution.py:500
  163.7 0.0 copy-start.2
  163.7 0.7 copy-done.2
  164.4 1.7 shard_map.111
  166.1 5.1 %all-to-all-start.5 = ((bf16[8,16,256]{2,1,0:T(8,128)(2,1)}), bf16[8,16,256]{2,1,0:T(8,128)(2,1)S(1)}, u32[]{:S(2)}, u32[]{:S(2)}) async-start(bf16[8,16,256]{2,1,0:T(8,128)(2,1)} %shard_map.111), calls=%async_computation.5 | async-start | bytes 131072 | tf_op jit(solution)/shard_map/all_to_all | solution.py:512
  171.2 0.0 collective-permute-done.11.rim_ref
  171.2 0.0 copy-start.6
  171.2 0.0 collective-permute-done.10.other_ref
  171.2 0.6 copy-done.6
  171.8 7.5 %shard_map.112 = (bf16[512,256]{1,0:T(8,128)(2,1)}, bf16[16,256]{1,0:T(8,128)(2,1)}, f32[512,256]{1,0:T(8,128)}, f32[512,256]{1,0:T(8,128)}) custom-call(s32[6]{0:T(128)} %stack.57.info_ref, bf16[512,2048]{1,0:T(8,128)(2,1)} %get-tuple-element.25.normed_ref, bf16[4,4,4,16,1024]{4,3,2,1,0:T(8,128)(2,1)} %copy-done, ...), custom_call_target="tpu_custom_call" | custom-call | flops 1073741824 | bytes 8388608 | tf_op jit(solution)/shard_map/pallas_call | solution.py:375
  179.3 2.0 shard_map.113.pool_ref
  181.3 0.0 all-to-all-done.5
  181.3 0.0 copy-start.5
  181.3 0.6 copy-done.5
  182.0 5.7 %shard_map.114 = bf16[512,2048]{1,0:T(8,128)(2,1)} custom-call(s32[6]{0:T(128)} %stack.57.info_ref, bf16[128,256]{1,0:T(8,128)(2,1)} %bitcast.26, f32[4,128,256]{2,1,0:T(8,128)} %get-tuple-element.23.growth_ref, f32[512,256]{1,0:T(8,128)} %get-tuple-element.24.cum_ref, f32[512,256]{1,0:T(8,128)} %get-tuple-element.29.decayed_ref, ...), custom_call_target="tpu_custom_call" | custom-call | flops 1073741824 | bytes 8388608 | tf_op jit(solution)/shard_map/pallas_call | solution.py:375
  187.6 31.6 %all_to_all.40 = bf16[4,128,2048]{2,1,0:T(8,128)(2,1)S(1)} all-to-all(bf16[4,128,2048]{2,1,0:T(8,128)(2,1)} %bitcast.23), channel_id=1, replica_groups=mesh['sp_f'=4,'sp_n'=4,'sp_x'=4,'sp_c'=2,'tp'=4] {'tp'}, dimensions={0} | all-to-all | bytes 4194304 | tf_op jit(solution)/shard_map/all_to_all | solution.py:566
  219.2 1.3 reduce_sum.12
  (3 shorter events, 0.0 us)
Async XLA Ops:
  33.4 30.6 %all-to-all-start.1 = ((bf16[4,4,16,512]{3,2,1,0:T(8,128)(2,1)}), bf16[4,4,16,512]{3,2,1,0:T(8,128)(2,1)S(1)}, u32[]{:S(2)}, u32[]{:S(2)}) async-start(bf16[4,4,16,512]{3,2,1,0:T(8,128)(2,1)} %broadcast_in_dim.20), calls=%async_computation.1 | async-start | bytes 524288 | tf_op jit(solution)/shard_map/all_to_all | solution.py:49
  38.0 14.2 %collective-permute-start.6 = (bf16[4,16,1024]{2,1,0:T(8,128)(2,1)S(1)}, bf16[4,16,1024]{2,1,0:T(8,128)(2,1)S(1)}, u32[]{:S(2)}, u32[]{:S(2)}) collective-permute-start(bf16[4,16,1024]{2,1,0:T(8,128)(2,1)S(1)} %get-tuple-element.36), channel_id=1, source_target_pairs={{0,448},{32,480},{64,0},{96,32},{128,64},{160,96},{192,128},{224,1... | collective-permute-start | bytes 393224 | tf_op jit(solution)/shard_map/ppermute | solution.py:56
  42.2 10.1 %collective-permute-start.5 = (bf16[4,16,1024]{2,1,0:T(8,128)(2,1)S(1)}, bf16[4,16,1024]{2,1,0:T(8,128)(2,1)S(1)}, u32[]{:S(2)}, u32[]{:S(2)}) collective-permute-start(bf16[4,16,1024]{2,1,0:T(8,128)(2,1)S(1)} %get-tuple-element.36), channel_id=1, source_target_pairs={{0,480},{32,0},{64,32},{96,64},{128,96},{160,128},{192,160},{224,1... | collective-permute-start | bytes 393224 | tf_op jit(solution)/shard_map/ppermute | solution.py:56
  44.7 8.1 %collective-permute-start.4 = (bf16[4,16,1024]{2,1,0:T(8,128)(2,1)S(1)}, bf16[4,16,1024]{2,1,0:T(8,128)(2,1)S(1)}, u32[]{:S(2)}, u32[]{:S(2)}) collective-permute-start(bf16[4,16,1024]{2,1,0:T(8,128)(2,1)S(1)} %get-tuple-element.36), channel_id=1, source_target_pairs={{0,32},{32,64},{64,96},{96,128},{128,160},{160,192},{192,224},{224... | collective-permute-start | bytes 393224 | tf_op jit(solution)/shard_map/ppermute | solution.py:56
  53.6 18.2 %collective-permute-start.9 = (bf16[4,4,16,1024]{3,2,1,0:T(8,128)(2,1)S(1)}, bf16[4,4,16,1024]{3,2,1,0:T(8,128)(2,1)S(1)}, u32[]{:S(2)}, u32[]{:S(2)}) collective-permute-start(bf16[4,4,16,1024]{3,2,1,0:T(8,128)(2,1)S(1)} %get-tuple-element.34), channel_id=1, source_target_pairs={{0,16},{8,24},{16,0},{24,8},{1,17},{9,25},{17,1},{25,9},{2,18},{10... | collective-permute-start | bytes 1572872 | tf_op jit(solution)/shard_map/ppermute | solution.py:56
  56.9 23.6 %collective-permute-start.8 = (bf16[4,4,16,1024]{3,2,1,0:T(8,128)(2,1)S(1)}, bf16[4,4,16,1024]{3,2,1,0:T(8,128)(2,1)S(1)}, u32[]{:S(2)}, u32[]{:S(2)}) collective-permute-start(bf16[4,4,16,1024]{3,2,1,0:T(8,128)(2,1)S(1)} %get-tuple-element.34), channel_id=1, source_target_pairs={{0,24},{8,0},{16,8},{24,16},{1,25},{9,1},{17,9},{25,17},{2,26},{10... | collective-permute-start | bytes 1572872 | tf_op jit(solution)/shard_map/ppermute | solution.py:56
  58.9 22.1 %collective-permute-start.7 = (bf16[4,4,16,1024]{3,2,1,0:T(8,128)(2,1)S(1)}, bf16[4,4,16,1024]{3,2,1,0:T(8,128)(2,1)}, u32[]{:S(2)}, u32[]{:S(2)}) collective-permute-start(bf16[4,4,16,1024]{3,2,1,0:T(8,128)(2,1)S(1)} %get-tuple-element.34), channel_id=1, source_target_pairs={{0,8},{8,16},{16,24},{24,0},{1,9},{9,17},{17,25},{25,1},{2,10},{10... | collective-permute-start | bytes 1572872 | tf_op jit(solution)/shard_map/ppermute | solution.py:56
  65.2 25.4 %all-to-all-start.2 = ((bf16[4,4,4,16,512]{4,3,2,1,0:T(8,128)(2,1)}), bf16[4,4,4,16,512]{4,3,2,1,0:T(8,128)(2,1)S(1)}, u32[]{:S(2)}, u32[]{:S(2)}) async-start(bf16[4,4,4,16,512]{4,3,2,1,0:T(8,128)(2,1)} %broadcast_in_dim.21), calls=%async_computation.2 | async-start | bytes 2097152 | tf_op jit(solution)/shard_map/all_to_all | solution.py:49
  71.8 9.1 %copy-start.3 = (bf16[4,4,16,1024]{3,2,1,0:T(8,128)(2,1)}, bf16[4,4,16,1024]{3,2,1,0:T(8,128)(2,1)S(1)}, u32[]{:S(2)}) copy-start(bf16[4,4,16,1024]{3,2,1,0:T(8,128)(2,1)S(1)} %collective-permute-done.9) | copy-start | bytes 1572868
  80.5 0.8 copy-start.4
  83.1 47.4 %copy-start = (bf16[4,4,4,16,1024]{4,3,2,1,0:T(8,128)(2,1)}, bf16[4,4,4,16,1024]{4,3,2,1,0:T(8,128)(2,1)S(1)}, u32[]{:S(2)}) copy-start(bf16[4,4,4,16,1024]{4,3,2,1,0:T(8,128)(2,1)S(1)} %pad_maximum_fusion.mine_ref) | copy-start | bytes 6291460
  83.1 88.1 %collective-permute-start.10 = (bf16[4,4,4,16,1024]{4,3,2,1,0:T(8,128)(2,1)S(1)}, bf16[4,4,4,16,1024]{4,3,2,1,0:T(8,128)(2,1)}, u32[]{:S(2)}, u32[]{:S(2)}) collective-permute-start(bf16[4,4,4,16,1024]{4,3,2,1,0:T(8,128)(2,1)S(1)} %pad_maximum_fusion.mine_ref), channel_id=1, source_target_pairs={{0,4},{4,0},{1,5},{5,1},{2,6},{6,2},{3,7},{7,3},{8,12},{12,8},{9,1... | collective-permute-start | bytes 6291464 | tf_op jit(solution)/shard_map/ppermute | solution.py:400
  90.6 32.2 %copy-start.1 = (bf16[4,4,4,16,512]{4,3,2,1,0:T(8,128)(2,1)}, bf16[4,4,4,16,512]{4,3,2,1,0:T(8,128)(2,1)S(1)}, u32[]{:S(2)}) copy-start(bf16[4,4,4,16,512]{4,3,2,1,0:T(8,128)(2,1)S(1)} %all-to-all-done.2.mine_ref) | copy-start | bytes 3145732
  90.6 32.1 %collective-permute-start.3 = (bf16[4,4,4,16,512]{4,3,2,1,0:T(8,128)(2,1)S(1)}, bf16[4,4,4,16,512]{4,3,2,1,0:T(8,128)(2,1)}, u32[]{:S(2)}, u32[]{:S(2)}) collective-permute-start(bf16[4,4,4,16,512]{4,3,2,1,0:T(8,128)(2,1)S(1)} %all-to-all-done.2.mine_ref), channel_id=1, source_target_pairs={{0,4},{4,0},{1,5},{5,1},{2,6},{6,2},{3,7},{7,3},{8,12},{12,8},{9,1... | collective-permute-start | bytes 3145736 | tf_op jit(solution)/shard_map/ppermute | solution.py:400
  92.5 17.8 %collective-permute-start = (bf16[128,2048]{1,0:T(8,128)(2,1)}, bf16[128,2048]{1,0:T(8,128)(2,1)}, u32[]{:S(2)}, u32[]{:S(2)}) collective-permute-start(bf16[128,2048]{1,0:T(8,128)(2,1)} %own_ref.1), channel_id=1, source_target_pairs={{0,1},{1,2},{2,3},{3,0},{4,5},{5,6},{6,7},{7,4},{8,9},{9,10},{10,1... | collective-permute-start | bytes 1572872 | tf_op jit(solution)/shard_map/ppermute | solution.py:56
  96.0 17.0 %collective-permute-start.1 = (bf16[128,2048]{1,0:T(8,128)(2,1)}, bf16[128,2048]{1,0:T(8,128)(2,1)}, u32[]{:S(2)}, u32[]{:S(2)}) collective-permute-start(bf16[128,2048]{1,0:T(8,128)(2,1)} %own_ref.1), channel_id=1, source_target_pairs={{0,3},{1,0},{2,1},{3,2},{4,7},{5,4},{6,5},{7,6},{8,11},{9,8},{10,9... | collective-permute-start | bytes 1572872 | tf_op jit(solution)/shard_map/ppermute | solution.py:56
  99.6 23.2 %collective-permute-start.2 = (bf16[128,2048]{1,0:T(8,128)(2,1)}, bf16[128,2048]{1,0:T(8,128)(2,1)}, u32[]{:S(2)}, u32[]{:S(2)}) collective-permute-start(bf16[128,2048]{1,0:T(8,128)(2,1)} %own_ref.1), channel_id=1, source_target_pairs={{0,2},{1,3},{2,0},{3,1},{4,6},{5,7},{6,4},{7,5},{8,10},{9,11},{10,... | collective-permute-start | bytes 1572872 | tf_op jit(solution)/shard_map/ppermute | solution.py:56
  140.8 22.9 %all-to-all-start.4 = ((bf16[16,24,256]{2,1,0:T(8,128)(2,1)}), bf16[16,24,256]{2,1,0:T(8,128)(2,1)S(1)}, u32[]{:S(2)}, u32[]{:S(2)}) async-start(bf16[16,24,256]{2,1,0:T(8,128)(2,1)} %get-tuple-element.20), calls=%async_computation.4 | async-start | bytes 393216 | tf_op jit(solution)/shard_map/all_to_all | solution.py:500
  147.2 23.9 %collective-permute-start.11 = (bf16[16,2048]{1,0:T(8,128)(2,1)}, bf16[16,2048]{1,0:T(8,128)(2,1)S(1)}, u32[]{:S(2)}, u32[]{:S(2)}) collective-permute-start(bf16[16,2048]{1,0:T(8,128)(2,1)} %get-tuple-element.28), channel_id=1, source_target_pairs={{0,4},{4,8},{8,12},{12,16},{16,20},{20,24},{24,28},{28,32},{32,36}... | collective-permute-start | bytes 196616 | tf_op jit(solution)/shard_map/ppermute | solution.py:486
  163.7 0.7 copy-start.2
  166.1 15.3 %all-to-all-start.5 = ((bf16[8,16,256]{2,1,0:T(8,128)(2,1)}), bf16[8,16,256]{2,1,0:T(8,128)(2,1)S(1)}, u32[]{:S(2)}, u32[]{:S(2)}) async-start(bf16[8,16,256]{2,1,0:T(8,128)(2,1)} %shard_map.111), calls=%async_computation.5 | async-start | bytes 131072 | tf_op jit(solution)/shard_map/all_to_all | solution.py:512
  171.2 0.6 copy-start.6
  181.3 0.6 copy-start.5
